TPU v7x, 512 devices: a whole 4x4x16 slice. The times are simulated.
512 devices in a mesh: pp: 16 (over z), fs: 4 (over y), tp: 8 (over x, core).
Axes of the slice: x: 4, y: 4, z: 16, core: 2. Of those that a mesh axis runs over, the one named last changes fastest.
Arguments:
- tokens: bfloat16 [16, 512, 1024], P('pp', 'fs', 'tp'), parts along dimension 1, may hold values from -640 to 640
- query_matrix: bfloat16 [16, 1024, 1024], P('pp', None, 'tp'), may hold values from -0.1875 to 0.1875
- key_matrix: bfloat16 [16, 1024, 1024], P('pp', None, 'tp'), may hold values from -0.1875 to 0.1875
- value_matrix: bfloat16 [16, 1024, 1024], P('pp', None, 'tp'), may hold values from -0.1875 to 0.1875
- output_gate_weight: bfloat16 [16, 1024, 1024], P('pp', None, 'tp'), may hold values from -0.1875 to 0.1875
- strength_weight: bfloat16 [16, 1024, 8], P('pp', None, 'tp'), may hold values from -0.1875 to 0.1875
- decay_input_weight: bfloat16 [16, 1024, 8], P('pp', None, 'tp'), may hold values from -0.1875 to 0.1875
- decay_scale_table: float32 [16, 8], P('pp', 'tp'), may hold values from 0.00078125 to 0.234375
- log_spike_decay: float32 [16, 128, 8], P('pp', None, 'tp'), may hold values from -2.1 to 0
- head_norm_gain: float32 [16, 1024], P('pp', 'tp'), may hold values from 0.1 to 1.9
- closing_norm_gain: float32 [1024], P('tp'), may hold values from 0.1 to 1.9
Outputs:
- normalized: bfloat16 [16, 512, 1024], P('pp', 'fs', 'tp'), parts along dimension 1
There are 4 independent parts, one for each index of `fs`. A program takes and returns all parts, laid end to end along the dimension named above; an argument that names none is the same for every part. Nothing has to cross between parts.
All inputs are finite; a program needn't handle non-finite values.
Results may differ from a plain program's by a relative error of at most 0.012.
Values may be sent and summed in bfloat16 or wider, within the bound.
No kernel may reach another device: no remote copies, remote signals or barrier semaphores. Data moves between devices by JAX's collectives and lax.ppermute only.
A program may use at most 64 MiB of HBM per device.

v0:
```python
import jax
import jax.numpy as jnp
from jax import lax
from jax.sharding import PartitionSpec as P

BLOCK = 64


epsilon = 1e-06


def from_behind(block, axis, distance):
    devices = range(lax.axis_size(axis))
    route = [((i - distance) % len(devices), i) for i in devices]
    return lax.ppermute(block, axis, route)


def from_everyone(shard, axis):
    copies = jnp.broadcast_to(shard, (lax.axis_size(axis), *shard.shape))
    return lax.all_to_all(copies, axis, split_axis=0, concat_axis=0, tiled=True)


def in_order(pieces, dim):
    shape = list(pieces.shape[1:])
    shape[dim] *= pieces.shape[0]
    return jnp.moveaxis(pieces, 0, dim).reshape(shape)


def gather_directly(shard, axis, dim):
    pieces = from_everyone(shard, axis)
    return in_order(pieces, dim)


def taken_together(shard, axis):
    everything = from_everyone(shard, axis)
    return jnp.sum(everything, axis=0)


def unit_lower_inverse(system):
    best_precision = lax.Precision.DEFAULT
    leading = system.shape[:-2]
    lead_count = len(leading)
    order = system.shape[-1]
    inverse = jnp.ones(leading + (order, 1, 1), jnp.float32)
    span = 1
    while span < order:
        count = order // (2 * span)
        tiles = system.reshape(leading + (count, 2 * span, count, 2 * span))
        diagonal_tiles = jnp.diagonal(tiles, axis1=lead_count, axis2=lead_count + 2)
        diagonal_tiles = jnp.moveaxis(diagonal_tiles, -1, lead_count)
        lower_left = diagonal_tiles[..., span:, :span]
        paired = inverse.reshape(leading + (count, 2, span, span))
        first = paired[..., 0, :, :]
        second = paired[..., 1, :, :]
        partial_left = jnp.einsum("...ij,...jk->...ik", lower_left, first, precision=best_precision)
        corner = -jnp.einsum("...ij,...jk->...ik", second, partial_left, precision=best_precision)
        top = jnp.concatenate([first, jnp.zeros_like(first)], axis=-1)
        bottom = jnp.concatenate([corner, second], axis=-1)
        inverse = jnp.concatenate([top, bottom], axis=-2)
        span = span * 2
    return inverse[..., 0, :, :]


def delta_rule(queries, keys_unit, values, beta_gate, decay_logarithm):
    length, head_count, head_width = queries.shape
    value_width = values.shape[-1]
    num_blocks = length // BLOCK
    best_precision = lax.Precision.DEFAULT

    def to_blocks(tensor):
        return tensor.reshape(num_blocks, BLOCK, head_count, -1).transpose(2, 0, 1, 3)

    query_b = to_blocks(queries)
    keys_b = to_blocks(keys_unit)
    values_b = to_blocks(values)
    beta_b = beta_gate.reshape(num_blocks, BLOCK, head_count).transpose(2, 0, 1)
    decay_b = decay_logarithm.reshape(num_blocks, BLOCK, head_count).transpose(2, 0, 1)
    cumulative = jnp.cumsum(decay_b, axis=-1)
    row_ids = lax.broadcasted_iota(jnp.int32, (BLOCK, BLOCK), 0)
    col_ids = lax.broadcasted_iota(jnp.int32, (BLOCK, BLOCK), 1)
    within = jnp.where(
        row_ids >= col_ids, cumulative[..., :, None] - cumulative[..., None, :], -jnp.inf
    )
    weights = jnp.exp(within)
    keys_beta = keys_b * beta_b[..., None]
    self_term = jnp.where(
        row_ids > col_ids,
        jnp.einsum("hnik,hnjk->hnij", keys_beta, keys_b, precision=best_precision) * weights,
        0.0,
    )
    system = self_term + jnp.eye(BLOCK, dtype=self_term.dtype)
    right_side = jnp.concatenate(
        [values_b * beta_b[..., None], keys_beta * jnp.exp(cumulative)[..., None]], axis=-1
    )
    inverse = unit_lower_inverse(system)
    solved = jnp.einsum("hnij,hnjc->hnic", inverse, right_side, precision=best_precision)
    update = solved[..., :value_width]
    correct = solved[..., value_width:]
    scores = jnp.einsum("hnik,hnjk->hnij", query_b, keys_b, precision=best_precision) * weights
    query_dec = query_b * jnp.exp(cumulative)[..., None]
    keys_dec = keys_b * jnp.exp(cumulative[..., -1:] - cumulative)[..., None]
    block_decay = jnp.exp(cumulative[..., -1])

    def advance(state_matrix, inputs):
        (
            state_update,
            correction_term,
            normed_queries,
            normed_keys,
            attention_scores,
            decay_factor,
        ) = inputs
        new_state = state_update - jnp.einsum(
            "rna,raq->rnq", correction_term, state_matrix, precision=best_precision
        )
        normed_output = jnp.einsum(
            "rna,raq->rnq", normed_queries, state_matrix, precision=best_precision
        ) + jnp.einsum("pak,pkr->par", attention_scores, new_state, precision=best_precision)
        state_matrix = state_matrix * decay_factor[:, None, None] + jnp.einsum(
            "fni,fnl->fil", normed_keys, new_state, precision=best_precision
        )
        return (state_matrix, normed_output)

    sequence_in = tuple(
        (
            jnp.moveaxis(tensor, 1, 0)
            for tensor in (update, correct, query_dec, keys_dec, scores, block_decay)
        )
    )
    initial_state = jnp.zeros((head_count, head_width, value_width), jnp.float32)
    final_state, outputs = lax.scan(advance, initial_state, sequence_in)
    return outputs.transpose(0, 2, 1, 3).reshape(length, head_count, value_width)


def merge_head_outputs(
    query_projected,
    key_projected,
    value_projected,
    gate_logits,
    strength_logits,
    decay_logits,
    decay_speed,
    spike_log_values,
    gain_vector,
):
    length = query_projected.shape[0]
    head_count = strength_logits.shape[-1]
    head_width = query_projected.shape[1] // head_count

    def normalize(projected):
        activated = jax.nn.silu(projected).reshape(length, head_count, -1)
        return activated * lax.rsqrt(
            jnp.sum(activated * activated, axis=-1, keepdims=True) + epsilon
        )

    queries = normalize(query_projected) * head_width ** (-0.5)
    keys_unit = normalize(key_projected)
    values = jax.nn.silu(value_projected).reshape(length, head_count, -1)
    beta_gate = jax.nn.sigmoid(strength_logits)
    decay_logarithm = -decay_speed[None, :] * jax.nn.softplus(decay_logits) + spike_log_values
    mixed_out = delta_rule(queries, keys_unit, values, beta_gate, decay_logarithm)
    mixed_out = (
        mixed_out
        * lax.rsqrt(jnp.mean(mixed_out * mixed_out, axis=-1, keepdims=True) + epsilon)
        * gain_vector.reshape(head_count, -1)
        * jax.nn.silu(gate_logits).reshape(length, head_count, -1)
    )
    return mixed_out.reshape(length, -1).astype(jnp.bfloat16)


def on_device(
    tokens,
    query_matrix,
    key_matrix,
    value_matrix,
    output_gate_weight,
    strength_weight,
    decay_input_weight,
    decay_scale_table,
    log_spike_decay,
    head_norm_gain,
    closing_norm_gain,
):
    section_count = lax.axis_size("pp")
    position = lax.axis_index("pp")
    matrices = (
        query_matrix[0],
        key_matrix[0],
        value_matrix[0],
        output_gate_weight[0],
        strength_weight[0],
        decay_input_weight[0],
    )
    decay_speed = decay_scale_table[0]
    spike_log_values = log_spike_decay[0]
    gain_vector = head_norm_gain[0]
    model_width = matrices[0].shape[0]
    row_count = tokens.shape[1]

    def is_active(step_index):
        offset = step_index - position
        return (offset >= 0) & (offset < section_count)

    def heads_of(projected):
        return merge_head_outputs(
            projected[0],
            projected[1],
            projected[2],
            projected[3],
            projected[4],
            projected[5],
            decay_speed,
            spike_log_values,
            gain_vector,
        )

    def advance_columns(step_index, carried):
        arriving = from_behind(carried, "pp", 1)
        initial = tuple(
            (jnp.zeros((row_count, matrix.shape[1]), jnp.float32) for matrix in matrices)
        )
        initial = initial + (jnp.zeros((row_count, 1), jnp.float32),)
        piece = gather_directly(arriving, "tp", 1)
        square = piece.astype(jnp.float32)
        sums = tuple(
            (jnp.dot(piece, matrix, preferred_element_type=jnp.float32) for matrix in matrices)
        )
        totals = sums + (jnp.sum(square * square, axis=1, keepdims=True),)
        inv_rms = lax.rsqrt(totals[-1] / model_width + epsilon)
        projected = [total * inv_rms for total in totals[:-1]]
        head_out = heads_of(projected)
        updated = (arriving.astype(jnp.float32) + head_out.astype(jnp.float32)).astype(jnp.bfloat16)
        return jnp.where(is_active(step_index), updated, arriving)

    own_columns = lax.fori_loop(0, 2 * section_count - 1, advance_columns, tokens[0])
    placed = from_behind(own_columns, "pp", 1)
    square = placed.astype(jnp.float32)
    row_total = taken_together(jnp.sum(square * square, axis=1), "tp")
    inv_rms = lax.rsqrt(row_total / model_width + epsilon)[:, None]
    normalized = (square * inv_rms * closing_norm_gain[None, :]).astype(jnp.bfloat16)
    return normalized[None]


def solution(mesh):
    placed = (
        P("pp", "fs", "tp"),
        P("pp", None, "tp"),
        P("pp", None, "tp"),
        P("pp", None, "tp"),
        P("pp", None, "tp"),
        P("pp", None, "tp"),
        P("pp", None, "tp"),
        P("pp", "tp"),
        P("pp", None, "tp"),
        P("pp", "tp"),
        P("tp"),
    )
    return jax.shard_map(
        on_device, mesh=mesh, in_specs=placed, out_specs=P("pp", "fs", "tp"), check_vma=False
    )
```

profile of v0, /device:TPU:1, one launch (start us, length us, event | category | flops | bytes accessed | tf_op | source)
XLA Modules:
  0.0 1359.8 jit_solution(9855434532946056933)
XLA Ops:
  1.4 1342.4 %while.47 = (s32[]{:T(128)}, bf16[128,128]{1,0:T(8,128)(2,1)S(1)}, s32[]{:T(128)}, bf16[1024,128]{1,0:T(8,128)(2,1)}, bf16[1024,1]{0,1:T(2,128)(2,1)}, /*index=5...) while((s32[]{:T(128)}, bf16[128,128]{1,0:T(8,128)(2,1)S(1)}, ...), condition=%wide.region_8.9_spmd, body=%wide.region_0.8_spmd.sunk | while | flops 152473792 | bytes 10487488 | solution.py:235
  5.9 8.8 collective-permute-done
  15.5 5.8 all-to-all-start
  21.5 6.4 all-to-all-done
  58.9 5.5 all-to-all-start
  64.5 6.4 all-to-all-done
  102.0 5.5 all-to-all-start
  107.5 6.4 all-to-all-done
  145.0 5.5 all-to-all-start
  150.6 6.4 all-to-all-done
  188.1 5.5 all-to-all-start
  193.7 6.4 all-to-all-done
  231.1 5.5 all-to-all-start
  236.7 6.4 all-to-all-done
  274.2 5.5 all-to-all-start
  279.8 6.4 all-to-all-done
  317.3 5.5 all-to-all-start
  322.8 6.4 all-to-all-done
  360.3 5.5 all-to-all-start
  365.9 6.4 all-to-all-done
  403.4 5.5 all-to-all-start
  408.9 6.4 all-to-all-done
  446.4 5.5 all-to-all-start
  452.0 6.4 all-to-all-done
  489.5 5.5 all-to-all-start
  495.1 6.4 all-to-all-done
  532.5 5.5 all-to-all-start
  538.1 6.4 all-to-all-done
  575.6 5.5 all-to-all-start
  581.2 6.4 all-to-all-done
  624.2 6.4 all-to-all-done
  667.3 6.4 all-to-all-done
  710.3 6.4 all-to-all-done
  753.4 6.4 all-to-all-done
  796.5 6.4 all-to-all-done
  839.5 6.4 all-to-all-done
  882.6 6.4 all-to-all-done
  925.6 6.4 all-to-all-done
  968.7 6.4 all-to-all-done
  1011.7 6.4 all-to-all-done
  1054.8 6.4 all-to-all-done
  1097.9 6.4 all-to-all-done
  1140.9 6.4 all-to-all-done
  1184.0 6.4 all-to-all-done
  1227.0 6.4 all-to-all-done
  1270.1 6.4 all-to-all-done
  1313.1 6.4 all-to-all-done
  1349.9 9.1 all_to_all.18
  (3312 shorter events, 1172.1 us)
Async XLA Ops:
  1.4 13.2 collective-permute-start
  15.5 12.3 all-to-all-start
  58.9 12.0 all-to-all-start
  102.0 12.0 all-to-all-start
  145.0 12.0 all-to-all-start
  181.4 5.9 collective-permute-start
  188.1 12.0 all-to-all-start
  224.4 5.9 collective-permute-start
  231.1 12.0 all-to-all-start
  267.5 5.9 collective-permute-start
  274.2 12.0 all-to-all-start
  310.5 5.9 collective-permute-start
  317.3 12.0 all-to-all-start
  353.6 5.9 collective-permute-start
  360.3 12.0 all-to-all-start
  403.4 12.0 all-to-all-start
  446.4 12.0 all-to-all-start
  489.5 12.0 all-to-all-start
  525.8 5.9 collective-permute-start
  532.5 12.0 all-to-all-start
  568.9 5.9 collective-permute-start
  575.6 12.0 all-to-all-start
  611.9 5.9 collective-permute-start
  618.7 12.0 all-to-all-start
  655.0 5.9 collective-permute-start
  661.7 12.0 all-to-all-start
  698.0 5.9 collective-permute-start
  704.8 12.0 all-to-all-start
  741.1 5.9 collective-permute-start
  747.8 12.0 all-to-all-start
  790.9 12.0 all-to-all-start
  833.9 12.0 all-to-all-start
  877.0 12.0 all-to-all-start
  913.3 5.9 collective-permute-start
  920.1 12.0 all-to-all-start
  956.4 5.9 collective-permute-start
  963.1 12.0 all-to-all-start
  999.4 5.9 collective-permute-start
  1006.2 12.0 all-to-all-start
  1042.5 5.9 collective-permute-start
  1049.2 12.0 all-to-all-start
  1085.6 5.9 collective-permute-start
  1092.3 12.0 all-to-all-start
  1135.3 12.0 all-to-all-start
  1178.4 12.0 all-to-all-start
  1221.5 12.0 all-to-all-start
  1264.5 12.0 all-to-all-start
  1307.6 12.0 all-to-all-start
  (202 other events, 2841.5 us)
where the time goes:
time: 1370 us; the launch traced here: 1360 us
  local copies, waits for them, and re-layouts  492 us (36%)
  waiting for transfers between devices  328 us (24%)
  matrix products  237 us (17%)
  starting transfers between devices  235 us (17%)
  other arithmetic  43.6 us (3%)
  loops' own time  14.2 us (1%)
    reshape x310, local copies, waits for them, and re-layouts, unit_lower_inverse(): tiles = system.reshape(leading + (count, 2 * span, count, 2 * span))  210 us
    all_to_all x31, waiting for transfers between devices, from_everyone(): return lax.all_to_all(copies, axis, split_axis=0, concat_axis=0, tiled=True)  199 us
    all_to_all x31, starting transfers between devices, from_everyone(): return lax.all_to_all(copies, axis, split_axis=0, concat_axis=0, tiled=True)  171 us
    gather x248, local copies, waits for them, and re-layouts, unit_lower_inverse(): diagonal_tiles = jnp.diagonal(tiles, axis1=lead_count, axis2=lead_count + 2)  143 us
    ppermute x32, waiting for transfers between devices, from_behind(): return lax.ppermute(block, axis, route)  129 us
    dot_general x186, matrix products, advance_columns(): jnp.dot(piece, matrix, preferred_element_type=jnp.float32)  102 us
    ppermute x32, starting transfers between devices, from_behind(): return lax.ppermute(block, axis, route)  63.9 us
    dot_general x62, matrix products, advance(): jnp.einsum('fni,fnl->fil', normed_keys, new_state, precision=best_precision)  54.3 us
  transfers between devices with their start and end apart: 63, of which 63 were waited for; matrix products, arithmetic and copies ran while one was open for 0% of the time, Pallas kernels for 0%

commit v1 on v0

v1 whole, which is shorter than its diff:
```python
import jax
import jax.numpy as jnp
from jax import lax
from jax.experimental import pallas as pl
from jax.experimental.pallas import tpu as pltpu
from jax.sharding import PartitionSpec as P

epsilon = 1e-06
TILE = 32


def silu(a):
    return a / (1.0 + jnp.exp(-a))


def layer_kernel(x_ref, own_ref, weight_ref, table_ref, out_ref):
    rows, model_width = x_ref.shape
    width = own_ref.shape[1]
    bf16, f32 = jnp.bfloat16, jnp.float32
    contract_lanes = (((1,), (1,)), ((), ()))
    x = x_ref[...]
    x32 = x.astype(f32)
    inv_rms = lax.rsqrt(jnp.sum(x32 * x32, axis=1, keepdims=True) * (1.0 / model_width) + epsilon)
    projected = jnp.dot(x, weight_ref[0], preferred_element_type=f32) * inv_rms
    table = table_ref[0]
    vectors = jnp.concatenate([table, jnp.zeros_like(table)], axis=0).astype(bf16)
    logits = lax.dot_general(vectors, x, contract_lanes, preferred_element_type=f32)

    row = lax.broadcasted_iota(jnp.int32, (rows, rows), 0)
    col = lax.broadcasted_iota(jnp.int32, (rows, rows), 1)

    def to_row(column):
        return jnp.sum(jnp.where(row == col, column, 0.0), axis=0, keepdims=True)

    def to_column(line):
        return jnp.sum(jnp.where(row == col, line, 0.0), axis=1, keepdims=True)

    inv_rms_row = to_row(inv_rms)
    beta_row = 1.0 / (1.0 + jnp.exp(-(logits[0:1] * inv_rms_row)))
    decay_row = logits[1:2] * inv_rms_row
    spike_row = table[2:3, :rows]
    gain_row = table[3:4, :width]
    speed_row = table[4:5, :rows]
    softplus = jnp.maximum(decay_row, 0.0) + jnp.log(1.0 + jnp.exp(-jnp.abs(decay_row)))
    g_row = spike_row - speed_row * softplus
    beta = to_column(beta_row)
    cumulative = jnp.sum(jnp.where(row >= col, g_row, 0.0), axis=1, keepdims=True)
    decay = jnp.where(row >= col, jnp.exp(jnp.minimum(cumulative - to_row(cumulative), 0.0)), 0.0)

    query = silu(projected[:, :width])
    query = query * (lax.rsqrt(jnp.sum(query * query, axis=1, keepdims=True) + epsilon) * width**-0.5)
    key = silu(projected[:, width : 2 * width])
    key = key * lax.rsqrt(jnp.sum(key * key, axis=1, keepdims=True) + epsilon)
    value = silu(projected[:, 2 * width : 3 * width]) * beta
    gate = silu(projected[:, 3 * width :])

    key16 = key.astype(bf16)
    both = jnp.concatenate([key16, query.astype(bf16)], axis=0)
    products = lax.dot_general(both, key16, contract_lanes, preferred_element_type=f32)
    scores = (products[rows:] * decay).astype(bf16)
    system = jnp.where(row > col, products[:rows] * decay * beta, 0.0)

    tiles = rows // TILE
    same_tile = row // TILE == col // TILE
    diagonal = jnp.sum(jnp.where(same_tile, system, 0.0).reshape(tiles, TILE, rows), axis=0)
    lane = lax.broadcasted_iota(jnp.int32, (TILE, rows), 1)
    sub = lax.broadcasted_iota(jnp.int32, (TILE, rows), 0)
    first_lane = lane - lane % TILE
    pieces = [
        (sub[8 * i : 8 * i + 8] == (lane % TILE)[8 * i : 8 * i + 8]).astype(f32)
        for i in range(TILE // 8)
    ]
    for j in range(TILE - 1):
        pivot = pieces[j // 8][j % 8 : j % 8 + 1]
        for i in range(j // 8, TILE // 8):
            if j % 8 == 7 and i == j // 8:
                continue
            factor = jnp.take_along_axis(
                diagonal[8 * i : 8 * i + 8], first_lane[:8] + j, axis=1, mode="promise_in_bounds"
            )
            pieces[i] = pieces[i] - factor * pivot
    tile_inverse = jnp.concatenate(pieces, axis=0)
    block_inverse = jnp.where(
        same_tile, jnp.concatenate([tile_inverse] * tiles, axis=0), 0.0
    ).astype(bf16)
    below = jnp.where(row // TILE > col // TILE, system, 0.0).astype(bf16)
    first = jnp.dot(
        block_inverse,
        jnp.concatenate([below, value.astype(bf16)], axis=1),
        preferred_element_type=f32,
    )
    coupling = first[:, :rows].astype(bf16)
    solved = first[:, rows:]
    second = jnp.dot(
        coupling,
        jnp.concatenate([coupling, solved.astype(bf16)], axis=1),
        preferred_element_type=f32,
    )
    solved = solved - second[:, rows:]
    solved = solved + jnp.dot(
        second[:, :rows].astype(bf16), solved.astype(bf16), preferred_element_type=f32
    )
    delta = jnp.dot(scores, solved.astype(bf16), preferred_element_type=f32)
    delta = delta * lax.rsqrt(jnp.sum(delta * delta, axis=1, keepdims=True) * (1.0 / width) + epsilon)
    head_out = (delta * gain_row * gate).astype(bf16)
    out_ref[...] = (own_ref[...].astype(f32) + head_out.astype(f32)).astype(bf16)


def apply_layer(layer, everything, own, weights, tables, interpret=False):
    whole = lambda i: (0, 0)
    this_layer = lambda i: (layer, 0, 0)
    return pl.pallas_call(
        layer_kernel,
        grid=(1,),
        in_specs=[
            pl.BlockSpec(everything.shape, whole),
            pl.BlockSpec(own.shape, whole),
            pl.BlockSpec((1, *weights.shape[1:]), this_layer),
            pl.BlockSpec((1, *tables.shape[1:]), this_layer),
        ],
        out_specs=pl.BlockSpec(own.shape, whole),
        out_shape=jax.ShapeDtypeStruct(own.shape, own.dtype),
        interpret=interpret,
        name="layer",
    )(everything, own, weights, tables)


def on_device(
    tokens,
    query_matrix,
    key_matrix,
    value_matrix,
    output_gate_weight,
    strength_weight,
    decay_input_weight,
    decay_scale_table,
    log_spike_decay,
    head_norm_gain,
    closing_norm_gain,
):
    model_width = query_matrix.shape[1]
    layer_total = lax.axis_size("pp")
    packed = jnp.concatenate(
        [query_matrix[0], key_matrix[0], value_matrix[0], output_gate_weight[0]], axis=1
    )
    weights = lax.all_gather(packed, "pp", axis=0)

    def line(vector):
        vector = vector.reshape(1, -1).astype(jnp.float32)
        return jnp.pad(vector, ((0, 0), (0, model_width - vector.shape[1])))

    table = jnp.concatenate(
        [
            line(strength_weight[0]),
            line(decay_input_weight[0]),
            line(log_spike_decay[0]),
            line(head_norm_gain[0]),
            jnp.broadcast_to(decay_scale_table[0], (1, model_width)),
            jnp.zeros((3, model_width), jnp.float32),
        ],
        axis=0,
    )
    tables = lax.all_gather(table, "pp", axis=0)
    own = tokens[0]
    for layer in range(layer_total):
        everything = lax.all_gather(own, "tp", axis=1, tiled=True)
        own = apply_layer(layer, everything, own, weights, tables)
    everything = lax.all_gather(own, "tp", axis=1, tiled=True).astype(jnp.float32)
    inv_rms = lax.rsqrt(jnp.mean(everything * everything, axis=1, keepdims=True) + epsilon)
    normalized = own.astype(jnp.float32) * inv_rms * closing_norm_gain[None, :]
    return normalized.astype(jnp.bfloat16)[None]


def solution(mesh):
    placed = (
        P("pp", "fs", "tp"),
        P("pp", None, "tp"),
        P("pp", None, "tp"),
        P("pp", None, "tp"),
        P("pp", None, "tp"),
        P("pp", None, "tp"),
        P("pp", None, "tp"),
        P("pp", "tp"),
        P("pp", None, "tp"),
        P("pp", "tp"),
        P("tp"),
    )
    return jax.shard_map(
        on_device, mesh=mesh, in_specs=placed, out_specs=P("pp", "fs", "tp"), check_vma=False
    )
```

time: 1370 us -> 482 us (0.35)
  local copies, waits for them, and re-layouts: 492 us -> 0.09 us
  blocking collectives: 9.15 us -> 263 us
  matrix products: 237 us -> 0 us
  starting transfers between devices: 235 us -> 0.04 us
  waiting for transfers between devices: 328 us -> 144 us
  Pallas kernels: 0 us -> 56.2 us
  other arithmetic: 43.6 us -> 3.9 us
  loops' own time: 14.2 us -> 0 us
    all_gather x0 -> x18, blocking collectives: none -> 263 us  [the longest x16 213 us: on_device(): everything = lax.all_gather(own, 'tp', axis=1, tiled=True)]
    dot_general x682 -> x0, matrix products: 237 us -> none  [the longest x186 102 us: advance_columns(): jnp.dot(piece, matrix, preferred_element_type=jnp.float32)]
    reshape x372 -> x0, local copies, waits for them, and re-layouts: 216 us -> none  [the longest x310 210 us: unit_lower_inverse(): tiles = system.reshape(leading + (count, 2 * span, count, 2 * span))]
    all_to_all x31 -> x0, waiting for transfers between devices: 199 us -> none  [from_everyone(): return lax.all_to_all(copies, axis, split_axis=0, concat_axis=0, tiled=True)]
    all_to_all x31 -> x0, starting transfers between devices: 171 us -> none  [from_everyone(): return lax.all_to_all(copies, axis, split_axis=0, concat_axis=0, tiled=True)]
    all_gather x0 -> x1, waiting for transfers between devices: none -> 144 us  [on_device(): weights = lax.all_gather(packed, 'pp', axis=0)]
    gather x248 -> x0, local copies, waits for them, and re-layouts: 143 us -> none  [unit_lower_inverse(): diagonal_tiles = jnp.diagonal(tiles, axis1=lead_count, axis2=lead_count + 2)]
    ppermute x32 -> x0, waiting for transfers between devices: 129 us -> none  [from_behind(): return lax.ppermute(block, axis, route)]
  transfers between devices with their start and end apart: 63 -> 1, of which waited for: 63 -> 1; matrix products, arithmetic and copies ran while one was open for 0% -> 0% of each run, Pallas kernels for 0% -> 0%
where the time goes in v1:
time: 482 us; the launch traced here: 481 us
  blocking collectives  263 us (55%)
  waiting for transfers between devices  144 us (30%)
  Pallas kernels  56.2 us (12%)
  between operations  14.2 us (3%)
    all_gather x16, blocking collectives, on_device(): everything = lax.all_gather(own, 'tp', axis=1, tiled=True)  213 us
    all_gather x1, waiting for transfers between devices, on_device(): weights = lax.all_gather(packed, 'pp', axis=0)  144 us
    pallas_call x16, Pallas kernels, apply_layer(): pl.pallas_call(layer_kernel, grid=(1,), in_specs=[pl.BlockSpec(everything...  56.2 us
    all_gather x1, blocking collectives, on_device(): tables = lax.all_gather(table, 'pp', axis=0)  38 us
    all_gather x1, blocking collectives, on_device(): lax.all_gather(own, 'tp', axis=1, tiled=True).astype(jnp.float32)  11.7 us
  transfers between devices with their start and end apart: 1, of which 1 were waited for; matrix products, arithmetic and copies ran while one was open for 0% of the time, Pallas kernels for 0%

profile of v1, /device:TPU:1, one launch (start us, length us, event | category | flops | bytes accessed | tf_op | source)
XLA Modules:
  0.0 480.8 jit_solution(1169351396765969188)
XLA Ops:
  6.5 0.0 copy-start.4
  6.6 0.0 all-gather.5.cloned.1.call-start
  6.6 2.3 pad_maximum_fusion
  8.9 0.0 all-gather.5.cloned.1.call-update
  8.9 0.0 copy-done.4
  8.9 0.0 copy-done.5
  9.6 0.0 copy-done.1
  9.6 0.0 copy-done.2
  9.7 0.1 concatenate.7
  9.7 0.0 copy-done
  9.7 19.0 %all-gather = bf16[1,128,1024]{2,1,0:T(8,128)(2,1)} all-gather(bf16[1,128,128]{2,1,0:T(8,128)(2,1)S(1)} %copy-done), channel_id=2, replica_groups=mesh['pp'=16,'fs'=4,'tp'=8] {'tp'}, dimensions={2}, use_global_device_ids=true | all-gather | bytes 294912 | tf_op jit(solution)/shard_map/all_gather | solution.py:166
  28.8 38.0 %all-gather.2 = f32[128,1024]{1,0:T(8,128)} all-gather(f32[8,1024]{1,0:T(8,128)S(1)} %concatenate.7), channel_id=4, replica_groups=mesh['pp'=16,'fs'=4,'tp'=8] {'pp'}, dimensions={0}, use_global_device_ids=true | all-gather | bytes 557056 | tf_op jit(solution)/shard_map/all_gather | solution.py:163
  66.7 143.6 %all-gather.5.cloned.1.call-done = bf16[16384,512]{1,0:T(8,128)(2,1)} async-done(((bf16[1024,512]{1,0:T(8,128)(2,1)}), bf16[16384,512]{1,0:T(8,128)(2,1)}) %all-gather.5.cloned.1.call-update) | async-done | bytes 16777232 | tf_op jit(solution)/shard_map/all_gather | solution.py:146
  210.4 3.5 layer.16.own_ref
  213.9 13.8 %all_gather.68.x_ref = bf16[128,1024]{1,0:T(8,128)(2,1)} all-gather(bf16[128,128]{1,0:T(8,128)(2,1)} %layer.16.own_ref), channel_id=1, replica_groups=mesh['pp'=16,'fs'=4,'tp'=8] {'tp'}, dimensions={1}, use_global_device_ids=true | all-gather | bytes 294912 | tf_op jit(solution)/shard_map/all_gather | solution.py:166
  227.7 3.5 layer.17.own_ref
  231.2 12.6 %all_gather.69.x_ref = bf16[128,1024]{1,0:T(8,128)(2,1)} all-gather(bf16[128,128]{1,0:T(8,128)(2,1)} %layer.17.own_ref), channel_id=1, replica_groups=mesh['pp'=16,'fs'=4,'tp'=8] {'tp'}, dimensions={1}, use_global_device_ids=true | all-gather | bytes 294912 | tf_op jit(solution)/shard_map/all_gather | solution.py:166
  243.8 3.5 layer.18.own_ref
  247.3 13.1 %all_gather.70.x_ref = bf16[128,1024]{1,0:T(8,128)(2,1)} all-gather(bf16[128,128]{1,0:T(8,128)(2,1)} %layer.18.own_ref), channel_id=1, replica_groups=mesh['pp'=16,'fs'=4,'tp'=8] {'tp'}, dimensions={1}, use_global_device_ids=true | all-gather | bytes 294912 | tf_op jit(solution)/shard_map/all_gather | solution.py:166
  260.4 3.5 layer.19.own_ref
  263.9 12.6 %all_gather.71.x_ref = bf16[128,1024]{1,0:T(8,128)(2,1)} all-gather(bf16[128,128]{1,0:T(8,128)(2,1)} %layer.19.own_ref), channel_id=1, replica_groups=mesh['pp'=16,'fs'=4,'tp'=8] {'tp'}, dimensions={1}, use_global_device_ids=true | all-gather | bytes 294912 | tf_op jit(solution)/shard_map/all_gather | solution.py:166
  276.5 3.5 layer.20.own_ref
  280.1 13.1 %all_gather.72.x_ref = bf16[128,1024]{1,0:T(8,128)(2,1)} all-gather(bf16[128,128]{1,0:T(8,128)(2,1)} %layer.20.own_ref), channel_id=1, replica_groups=mesh['pp'=16,'fs'=4,'tp'=8] {'tp'}, dimensions={1}, use_global_device_ids=true | all-gather | bytes 294912 | tf_op jit(solution)/shard_map/all_gather | solution.py:166
  293.1 3.5 layer.21.own_ref
  296.7 12.6 %all_gather.73.x_ref = bf16[128,1024]{1,0:T(8,128)(2,1)} all-gather(bf16[128,128]{1,0:T(8,128)(2,1)} %layer.21.own_ref), channel_id=1, replica_groups=mesh['pp'=16,'fs'=4,'tp'=8] {'tp'}, dimensions={1}, use_global_device_ids=true | all-gather | bytes 294912 | tf_op jit(solution)/shard_map/all_gather | solution.py:166
  309.3 3.5 layer.22.own_ref
  312.8 13.1 %all_gather.74.x_ref = bf16[128,1024]{1,0:T(8,128)(2,1)} all-gather(bf16[128,128]{1,0:T(8,128)(2,1)} %layer.22.own_ref), channel_id=1, replica_groups=mesh['pp'=16,'fs'=4,'tp'=8] {'tp'}, dimensions={1}, use_global_device_ids=true | all-gather | bytes 294912 | tf_op jit(solution)/shard_map/all_gather | solution.py:166
  325.9 3.5 layer.23.own_ref
  329.4 12.8 %all_gather.75.x_ref = bf16[128,1024]{1,0:T(8,128)(2,1)} all-gather(bf16[128,128]{1,0:T(8,128)(2,1)} %layer.23.own_ref), channel_id=1, replica_groups=mesh['pp'=16,'fs'=4,'tp'=8] {'tp'}, dimensions={1}, use_global_device_ids=true | all-gather | bytes 294912 | tf_op jit(solution)/shard_map/all_gather | solution.py:166
  342.2 3.5 layer.24.own_ref
  345.7 13.1 %all_gather.76.x_ref = bf16[128,1024]{1,0:T(8,128)(2,1)} all-gather(bf16[128,128]{1,0:T(8,128)(2,1)} %layer.24.own_ref), channel_id=1, replica_groups=mesh['pp'=16,'fs'=4,'tp'=8] {'tp'}, dimensions={1}, use_global_device_ids=true | all-gather | bytes 294912 | tf_op jit(solution)/shard_map/all_gather | solution.py:166
  358.8 3.5 layer.25.own_ref
  362.3 12.6 %all_gather.77.x_ref = bf16[128,1024]{1,0:T(8,128)(2,1)} all-gather(bf16[128,128]{1,0:T(8,128)(2,1)} %layer.25.own_ref), channel_id=1, replica_groups=mesh['pp'=16,'fs'=4,'tp'=8] {'tp'}, dimensions={1}, use_global_device_ids=true | all-gather | bytes 294912 | tf_op jit(solution)/shard_map/all_gather | solution.py:166
  375.0 3.5 layer.26.own_ref
  378.5 13.1 %all_gather.78.x_ref = bf16[128,1024]{1,0:T(8,128)(2,1)} all-gather(bf16[128,128]{1,0:T(8,128)(2,1)} %layer.26.own_ref), channel_id=1, replica_groups=mesh['pp'=16,'fs'=4,'tp'=8] {'tp'}, dimensions={1}, use_global_device_ids=true | all-gather | bytes 294912 | tf_op jit(solution)/shard_map/all_gather | solution.py:166
  391.6 3.5 layer.27.own_ref
  395.1 12.6 %all_gather.79.x_ref = bf16[128,1024]{1,0:T(8,128)(2,1)} all-gather(bf16[128,128]{1,0:T(8,128)(2,1)} %layer.27.own_ref), channel_id=1, replica_groups=mesh['pp'=16,'fs'=4,'tp'=8] {'tp'}, dimensions={1}, use_global_device_ids=true | all-gather | bytes 294912 | tf_op jit(solution)/shard_map/all_gather | solution.py:166
  407.7 3.5 layer.28.own_ref
  411.2 13.1 %all_gather.80.x_ref = bf16[128,1024]{1,0:T(8,128)(2,1)} all-gather(bf16[128,128]{1,0:T(8,128)(2,1)} %layer.28.own_ref), channel_id=1, replica_groups=mesh['pp'=16,'fs'=4,'tp'=8] {'tp'}, dimensions={1}, use_global_device_ids=true | all-gather | bytes 294912 | tf_op jit(solution)/shard_map/all_gather | solution.py:166
  424.3 3.5 layer.29.own_ref
  427.8 12.6 %all_gather.81.x_ref = bf16[128,1024]{1,0:T(8,128)(2,1)} all-gather(bf16[128,128]{1,0:T(8,128)(2,1)} %layer.29.own_ref), channel_id=1, replica_groups=mesh['pp'=16,'fs'=4,'tp'=8] {'tp'}, dimensions={1}, use_global_device_ids=true | all-gather | bytes 294912 | tf_op jit(solution)/shard_map/all_gather | solution.py:166
  440.4 3.5 layer.30.own_ref
  444.0 13.1 %all_gather.82.x_ref = bf16[128,1024]{1,0:T(8,128)(2,1)} all-gather(bf16[128,128]{1,0:T(8,128)(2,1)} %layer.30.own_ref), channel_id=1, replica_groups=mesh['pp'=16,'fs'=4,'tp'=8] {'tp'}, dimensions={1}, use_global_device_ids=true | all-gather | bytes 294912 | tf_op jit(solution)/shard_map/all_gather | solution.py:166
  457.1 3.5 layer.31
  460.6 11.7 %all_gather.83 = bf16[128,1024]{1,0:T(8,128)(2,1)S(1)} all-gather(bf16[128,128]{1,0:T(8,128)(2,1)} %layer.31), channel_id=1, replica_groups=mesh['pp'=16,'fs'=4,'tp'=8] {'tp'}, dimensions={1}, use_global_device_ids=true | all-gather | bytes 294912 | tf_op jit(solution)/shard_map/all_gather | solution.py:168
  472.3 0.1 multiply_reduce_fusion
  472.4 0.0 copy-done.3
  472.4 1.5 fusion
  (11 shorter events, 0.0 us)
Async XLA Ops:
  6.5 2.4 copy-start.4
  6.5 2.4 copy-start.5
  6.5 3.1 copy-start.1
  6.5 3.1 copy-start.2
  6.5 3.2 copy-start
  6.6 203.8 %all-gather.5.cloned.1.call-start = ((), (), s32[]{:S(2)}) async-start(), calls=%async_computation | async-start | bytes 17825792 | tf_op jit(solution)/shard_map/all_gather | solution.py:146
  457.1 15.4 %copy-start.3 = (f32[128]{0:T(128)S(1)}, f32[128]{0:T(128)}, u32[]{:S(2)}) copy-start(f32[128]{0:T(128)} %param.21) | copy-start | bytes 1540
Sparse Core Ops, SparseCore 0:
  9.4 200.8 all-gather.4

commit v2 on v1

--- a/solution.py
+++ b/solution.py
@@ -7,21 +7,32 @@
 
 epsilon = 1e-06
 TILE = 32
+GROUPS = (0, 1, 3, 7, 12, 16)
+DIRECT = 3
 
 
 def silu(a):
     return a / (1.0 + jnp.exp(-a))
 
 
-def layer_kernel(x_ref, own_ref, weight_ref, table_ref, out_ref):
-    rows, model_width = x_ref.shape
-    width = own_ref.shape[1]
+def layer_kernel(x_ref, own_ref, weight_ref, table_ref, out_ref, copies_ref):
+    rows, width = own_ref.shape
+    parts = weight_ref.shape[0]
+    part_width = weight_ref.shape[2]
+    model_width = parts * part_width
     bf16, f32 = jnp.bfloat16, jnp.float32
     contract_lanes = (((1,), (1,)), ((), ()))
-    x = x_ref[...]
+    x = jnp.concatenate([x_ref[i] for i in range(x_ref.shape[0])], axis=1)
     x32 = x.astype(f32)
     inv_rms = lax.rsqrt(jnp.sum(x32 * x32, axis=1, keepdims=True) * (1.0 / model_width) + epsilon)
-    projected = jnp.dot(x, weight_ref[0], preferred_element_type=f32) * inv_rms
+    projected = jnp.zeros((rows, weight_ref.shape[3]), f32)
+    for i in range(parts):
+        projected += jnp.dot(
+            x[:, i * part_width : (i + 1) * part_width],
+            weight_ref[i, 0],
+            preferred_element_type=f32,
+        )
+    projected = projected * inv_rms
     table = table_ref[0]
     vectors = jnp.concatenate([table, jnp.zeros_like(table)], axis=0).astype(bf16)
     logits = lax.dot_general(vectors, x, contract_lanes, preferred_element_type=f32)
@@ -103,26 +114,43 @@
     delta = jnp.dot(scores, solved.astype(bf16), preferred_element_type=f32)
     delta = delta * lax.rsqrt(jnp.sum(delta * delta, axis=1, keepdims=True) * (1.0 / width) + epsilon)
     head_out = (delta * gain_row * gate).astype(bf16)
-    out_ref[...] = (own_ref[...].astype(f32) + head_out.astype(f32)).astype(bf16)
-
-
-def apply_layer(layer, everything, own, weights, tables, interpret=False):
-    whole = lambda i: (0, 0)
-    this_layer = lambda i: (layer, 0, 0)
+    updated = (own_ref[...].astype(f32) + head_out.astype(f32)).astype(bf16)
+    out_ref[...] = updated
+    for i in range(copies_ref.shape[0]):
+        copies_ref[i] = updated
+
+
+def apply_layer(layer, place, everything, own, weights, tables, interpret=False):
+    parts, _, part_width, columns = weights.shape
     return pl.pallas_call(
         layer_kernel,
         grid=(1,),
         in_specs=[
-            pl.BlockSpec(everything.shape, whole),
-            pl.BlockSpec(own.shape, whole),
-            pl.BlockSpec((1, *weights.shape[1:]), this_layer),
-            pl.BlockSpec((1, *tables.shape[1:]), this_layer),
-        ],
-        out_specs=pl.BlockSpec(own.shape, whole),
-        out_shape=jax.ShapeDtypeStruct(own.shape, own.dtype),
+            pl.BlockSpec(everything.shape, lambda i: (0, 0, 0)),
+            pl.BlockSpec(own.shape, lambda i: (0, 0)),
+            pl.BlockSpec((parts, 1, part_width, columns), lambda i: (0, place, 0, 0)),
+            pl.BlockSpec((1, *tables.shape[1:]), lambda i: (layer, 0, 0)),
+        ],
+        out_specs=[
+            pl.BlockSpec(own.shape, lambda i: (0, 0)),
+            pl.BlockSpec(everything.shape, lambda i: (0, 0, 0)),
+        ],
+        out_shape=[
+            jax.ShapeDtypeStruct(own.shape, own.dtype),
+            jax.ShapeDtypeStruct(everything.shape, own.dtype),
+        ],
         interpret=interpret,
+        compiler_params=pltpu.CompilerParams(vmem_limit_bytes=12 * 1024 * 1024),
         name="layer",
     )(everything, own, weights, tables)
+
+
+def exchange(copies, axis):
+    return lax.all_to_all(copies, axis, split_axis=0, concat_axis=0, tiled=True)
+
+
+def from_everyone(shard, axis):
+    return exchange(jnp.broadcast_to(shard, (lax.axis_size(axis), *shard.shape)), axis)
 
 
 def on_device(
@@ -140,11 +168,15 @@
 ):
     model_width = query_matrix.shape[1]
     layer_total = lax.axis_size("pp")
+    part_rows = model_width // lax.axis_size("fs")
+    first_row = lax.axis_index("fs") * part_rows
     packed = jnp.concatenate(
-        [query_matrix[0], key_matrix[0], value_matrix[0], output_gate_weight[0]], axis=1
-    )
-    weights = lax.all_gather(packed, "pp", axis=0)
-
+        [
+            lax.dynamic_slice_in_dim(matrix[0], first_row, part_rows, axis=0)
+            for matrix in (query_matrix, key_matrix, value_matrix, output_gate_weight)
+        ],
+        axis=1,
+    )
     def line(vector):
         vector = vector.reshape(1, -1).astype(jnp.float32)
         return jnp.pad(vector, ((0, 0), (0, model_width - vector.shape[1])))
@@ -162,11 +194,25 @@
     )
     tables = lax.all_gather(table, "pp", axis=0)
     own = tokens[0]
+    everything = from_everyone(own, "tp")
+    quarters = lax.all_gather(packed, "pp", axis=0)
+    quarters, everything, tables = lax.optimization_barrier((quarters, everything, tables))
+    stored = {}
+    for begin, end in zip(GROUPS[:-1], GROUPS[1:]):
+        group = quarters[begin:end]
+        if begin < DIRECT:
+            group = from_everyone(group, "fs")
+        else:
+            group = lax.all_gather(group, "fs", axis=0)
+        for layer in range(begin, end):
+            stored[layer] = (layer - begin, group)
     for layer in range(layer_total):
-        everything = lax.all_gather(own, "tp", axis=1, tiled=True)
-        own = apply_layer(layer, everything, own, weights, tables)
-    everything = lax.all_gather(own, "tp", axis=1, tiled=True).astype(jnp.float32)
-    inv_rms = lax.rsqrt(jnp.mean(everything * everything, axis=1, keepdims=True) + epsilon)
+        place, weights = stored[layer]
+        own, copies = apply_layer(layer, place, everything, own, weights, tables)
+        everything = exchange(copies, "tp")
+    square = everything.astype(jnp.float32)
+    row_total = jnp.sum(jnp.sum(square * square, axis=0), axis=1, keepdims=True)
+    inv_rms = lax.rsqrt(row_total / model_width + epsilon)
     normalized = own.astype(jnp.float32) * inv_rms * closing_norm_gain[None, :]
     return normalized.astype(jnp.bfloat16)[None]
 

time: 482 us -> 364 us (0.76)
  waiting for transfers between devices: 144 us -> 45.5 us
  blocking collectives: 263 us -> 224 us
  starting transfers between devices: 0.04 us -> 30.8 us
  Pallas kernels: 56.2 us -> 26.7 us
  local copies, waits for them, and re-layouts: 0.09 us -> 19.4 us
    all_gather x17 -> x0, blocking collectives: 225 us -> none  [the longest x16 213 us: on_device(): everything = lax.all_gather(own, 'tp', axis=1, tiled=True)]
    all_to_all x0 -> x16, blocking collectives: none -> 194 us  [exchange(): return lax.all_to_all(copies, axis, split_axis=0, concat_axis=0, tiled=True)]
    all_gather x1 -> x4, waiting for transfers between devices: 144 us -> 33 us  [the longest x1 33 us: on_device(): quarters = lax.all_gather(packed, 'pp', axis=0)]
    all_to_all x0 -> x3, starting transfers between devices: none -> 30.7 us  [exchange(): return lax.all_to_all(copies, axis, split_axis=0, concat_axis=0, tiled=True)]
    pallas_call x16, Pallas kernels: 56.2 us -> 26.7 us  [apply_layer(): pl.pallas_call(layer_kernel, grid=(1,), in_specs=[pl.BlockSpec(everything...]
    all_to_all x0 -> x3, waiting for transfers between devices: none -> 11.9 us  [exchange(): return lax.all_to_all(copies, axis, split_axis=0, concat_axis=0, tiled=True)]
    all_gather x1, blocking collectives: 38 us -> 29.8 us  [on_device(): tables = lax.all_gather(table, 'pp', axis=0)]
    slice x0 -> x4, local copies, waits for them, and re-layouts: none -> 7.6 us  [on_device(): group = quarters[begin:end]]
  transfers between devices with their start and end apart: 1 -> 7, of which waited for: 1 -> 3; matrix products, arithmetic and copies ran while one was open for 0% -> 2% of each run, Pallas kernels for 0% -> 6%
where the time goes in v2:
time: 364 us; the launch traced here: 363 us
  blocking collectives  224 us (62%)
  waiting for transfers between devices  45.5 us (12%)
  starting transfers between devices  30.8 us (8%)
  Pallas kernels  26.7 us (7%)
  local copies, waits for them, and re-layouts  19.4 us (5%)
  between operations  14 us (4%)
    all_to_all x16, blocking collectives, exchange(): return lax.all_to_all(copies, axis, split_axis=0, concat_axis=0, tiled=True)  194 us
    all_gather x1, waiting for transfers between devices, on_device(): quarters = lax.all_gather(packed, 'pp', axis=0)  33 us
    all_to_all x3, starting transfers between devices, exchange(): return lax.all_to_all(copies, axis, split_axis=0, concat_axis=0, tiled=True)  30.7 us
    all_gather x1, blocking collectives, on_device(): tables = lax.all_gather(table, 'pp', axis=0)  29.8 us
    pallas_call x16, Pallas kernels, apply_layer(): pl.pallas_call(layer_kernel, grid=(1,), in_specs=[pl.BlockSpec(everything...  26.7 us
    all_to_all x3, waiting for transfers between devices, exchange(): return lax.all_to_all(copies, axis, split_axis=0, concat_axis=0, tiled=True)  11.9 us
    slice x4, local copies, waits for them, and re-layouts, on_device(): group = quarters[begin:end]  7.6 us
  transfers between devices with their start and end apart: 7, of which 3 were waited for; matrix products, arithmetic and copies ran while one was open for 2% of the time, Pallas kernels for 6%

profile of v2, /device:TPU:1, one launch (start us, length us, event | category | flops | bytes accessed | tf_op | source)
XLA Modules:
  0.0 362.6 jit_solution(1264485593978047720)
XLA Ops:
  7.4 0.9 dynamic-slice_bitcast_fusion.2
  9.1 1.5 broadcast_in_dim.22
  10.6 10.2 %all-to-all-start = ((bf16[8,128,128]{2,1,0:T(8,128)(2,1)}), bf16[8,128,128]{2,1,0:T(8,128)(2,1)S(1)}, u32[]{:S(2)}, u32[]{:S(2)}) async-start(bf16[8,128,128]{2,1,0:T(8,128)(2,1)} %broadcast_in_dim.22), calls=%async_computation | async-start | bytes 524288 | tf_op jit(solution)/shard_map/all_to_all | solution.py:149
  23.5 29.8 %all-gather.1 = f32[128,1024]{1,0:T(8,128)S(1)} all-gather(f32[8,1024]{1,0:T(8,128)S(1)} %concatenate.7), channel_id=3, replica_groups=mesh['pp'=16,'fs'=4,'tp'=8] {'pp'}, dimensions={0}, use_global_device_ids=true | all-gather | bytes 557056 | tf_op jit(solution)/shard_map/all_gather | solution.py:195
  53.3 33.0 %all-gather.10.cloned.1.call-done = bf16[4096,512]{1,0:T(8,128)(2,1)} async-done(((bf16[256,512]{1,0:T(8,128)(2,1)}), bf16[4096,512]{1,0:T(8,128)(2,1)}) %all-gather.10.cloned.1.call-update) | async-done | bytes 4194320 | tf_op jit(solution)/shard_map/all_gather | solution.py:198
  86.3 3.0 fusion.1
  89.4 2.5 slice.21
  92.5 1.0 slice_bitcast_fusion
  93.5 13.7 %all_to_all.95.weight_ref = bf16[4,1,256,512]{3,2,1,0:T(8,128)(2,1)S(1)} all-to-all(bf16[4,1,256,512]{3,2,1,0:T(8,128)(2,1)S(1)} %broadcast_in_dim.25), channel_id=1, replica_groups=mesh['pp'=16,'fs'=4,'tp'=8] {'fs'}, dimensions={0} | all-to-all | bytes 2097152 | tf_op jit(solution)/shard_map/all_to_all | solution.py:149
  107.2 2.3 layer.16
  109.5 16.3 %all-to-all-start.2 = ((bf16[8,128,128]{2,1,0:T(8,128)(2,1)}), bf16[8,128,128]{2,1,0:T(8,128)(2,1)S(1)}, u32[]{:S(2)}, u32[]{:S(2)}) async-start(bf16[8,128,128]{2,1,0:T(8,128)(2,1)} %get-tuple-element.43), calls=%async_computation.2 | async-start | bytes 524288 | tf_op jit(solution)/shard_map/all_to_all | solution.py:149
  125.8 1.1 slice.19
  126.9 5.4 %all-to-all-done.2.x_ref = bf16[8,128,128]{2,1,0:T(8,128)(2,1)S(1)} async-done(((bf16[8,128,128]{2,1,0:T(8,128)(2,1)}), bf16[8,128,128]{2,1,0:T(8,128)(2,1)S(1)}, u32[]{:S(2)}, u32[]{:S(2)}) %all-to-all-start.2) | async-done | bytes 262176 | tf_op jit(solution)/shard_map/all_to_all | solution.py:149
  132.5 39.6 %all_to_all.96.weight_ref = bf16[4,2,256,512]{3,2,1,0:T(8,128)(2,1)S(1)} all-to-all(bf16[4,2,256,512]{3,2,1,0:T(8,128)(2,1)S(1)} %broadcast_in_dim.26), channel_id=1, replica_groups=mesh['pp'=16,'fs'=4,'tp'=8] {'fs'}, dimensions={0} | all-to-all | bytes 4194304 | tf_op jit(solution)/shard_map/all_to_all | solution.py:149
  172.1 1.6 layer.17
  173.7 11.9 %all_to_all.97.x_ref = bf16[8,128,128]{2,1,0:T(8,128)(2,1)S(1)} all-to-all(bf16[8,128,128]{2,1,0:T(8,128)(2,1)S(1)} %get-tuple-element.45), channel_id=1, replica_groups=mesh['pp'=16,'fs'=4,'tp'=8] {'tp'}, dimensions={0} | all-to-all | bytes 524288 | tf_op jit(solution)/shard_map/all_to_all | solution.py:149
  185.6 1.6 layer.18
  187.2 10.0 %all_to_all.98.x_ref = bf16[8,128,128]{2,1,0:T(8,128)(2,1)S(1)} all-to-all(bf16[8,128,128]{2,1,0:T(8,128)(2,1)S(1)} %get-tuple-element.47), channel_id=1, replica_groups=mesh['pp'=16,'fs'=4,'tp'=8] {'tp'}, dimensions={0} | all-to-all | bytes 524288 | tf_op jit(solution)/shard_map/all_to_all | solution.py:149
  197.2 2.2 copy-done.4
  199.4 1.6 layer.19
  201.0 9.9 %all_to_all.99.x_ref = bf16[8,128,128]{2,1,0:T(8,128)(2,1)S(1)} all-to-all(bf16[8,128,128]{2,1,0:T(8,128)(2,1)S(1)} %get-tuple-element.49), channel_id=1, replica_groups=mesh['pp'=16,'fs'=4,'tp'=8] {'tp'}, dimensions={0} | all-to-all | bytes 524288 | tf_op jit(solution)/shard_map/all_to_all | solution.py:149
  210.9 1.6 layer.20
  212.5 9.9 %all_to_all.100.x_ref = bf16[8,128,128]{2,1,0:T(8,128)(2,1)S(1)} all-to-all(bf16[8,128,128]{2,1,0:T(8,128)(2,1)S(1)} %get-tuple-element.51), channel_id=1, replica_groups=mesh['pp'=16,'fs'=4,'tp'=8] {'tp'}, dimensions={0} | all-to-all | bytes 524288 | tf_op jit(solution)/shard_map/all_to_all | solution.py:149
  222.4 1.6 layer.21
  224.0 9.9 %all_to_all.101.x_ref = bf16[8,128,128]{2,1,0:T(8,128)(2,1)S(1)} all-to-all(bf16[8,128,128]{2,1,0:T(8,128)(2,1)S(1)} %get-tuple-element.53), channel_id=1, replica_groups=mesh['pp'=16,'fs'=4,'tp'=8] {'tp'}, dimensions={0} | all-to-all | bytes 524288 | tf_op jit(solution)/shard_map/all_to_all | solution.py:149
  233.9 1.6 layer.22
  235.5 9.9 %all_to_all.102.x_ref = bf16[8,128,128]{2,1,0:T(8,128)(2,1)S(1)} all-to-all(bf16[8,128,128]{2,1,0:T(8,128)(2,1)S(1)} %get-tuple-element.55), channel_id=1, replica_groups=mesh['pp'=16,'fs'=4,'tp'=8] {'tp'}, dimensions={0} | all-to-all | bytes 524288 | tf_op jit(solution)/shard_map/all_to_all | solution.py:149
  245.3 2.5 copy-done
  247.8 1.6 layer.23
  249.4 9.9 %all_to_all.103.x_ref = bf16[8,128,128]{2,1,0:T(8,128)(2,1)S(1)} all-to-all(bf16[8,128,128]{2,1,0:T(8,128)(2,1)S(1)} %get-tuple-element.57), channel_id=1, replica_groups=mesh['pp'=16,'fs'=4,'tp'=8] {'tp'}, dimensions={0} | all-to-all | bytes 524288 | tf_op jit(solution)/shard_map/all_to_all | solution.py:149
  259.3 1.6 layer.24
  260.9 10.0 %all_to_all.104.x_ref = bf16[8,128,128]{2,1,0:T(8,128)(2,1)S(1)} all-to-all(bf16[8,128,128]{2,1,0:T(8,128)(2,1)S(1)} %get-tuple-element.59), channel_id=1, replica_groups=mesh['pp'=16,'fs'=4,'tp'=8] {'tp'}, dimensions={0} | all-to-all | bytes 524288 | tf_op jit(solution)/shard_map/all_to_all | solution.py:149
  270.9 1.6 layer.25
  272.5 9.9 %all_to_all.105.x_ref = bf16[8,128,128]{2,1,0:T(8,128)(2,1)S(1)} all-to-all(bf16[8,128,128]{2,1,0:T(8,128)(2,1)S(1)} %get-tuple-element.61), channel_id=1, replica_groups=mesh['pp'=16,'fs'=4,'tp'=8] {'tp'}, dimensions={0} | all-to-all | bytes 524288 | tf_op jit(solution)/shard_map/all_to_all | solution.py:149
  282.4 1.6 layer.26
  284.0 9.9 %all_to_all.106.x_ref = bf16[8,128,128]{2,1,0:T(8,128)(2,1)S(1)} all-to-all(bf16[8,128,128]{2,1,0:T(8,128)(2,1)S(1)} %get-tuple-element.63), channel_id=1, replica_groups=mesh['pp'=16,'fs'=4,'tp'=8] {'tp'}, dimensions={0} | all-to-all | bytes 524288 | tf_op jit(solution)/shard_map/all_to_all | solution.py:149
  293.9 2.3 layer.27
  296.2 4.3 %all-to-all-start.14 = ((bf16[8,128,128]{2,1,0:T(8,128)(2,1)}), bf16[8,128,128]{2,1,0:T(8,128)(2,1)S(1)}, u32[]{:S(2)}, u32[]{:S(2)}) async-start(bf16[8,128,128]{2,1,0:T(8,128)(2,1)} %get-tuple-element.65), calls=%async_computation.14 | async-start | bytes 524288 | tf_op jit(solution)/shard_map/all_to_all | solution.py:149
  300.5 6.5 %all-to-all-done.14.x_ref = bf16[8,128,128]{2,1,0:T(8,128)(2,1)S(1)} async-done(((bf16[8,128,128]{2,1,0:T(8,128)(2,1)}), bf16[8,128,128]{2,1,0:T(8,128)(2,1)S(1)}, u32[]{:S(2)}, u32[]{:S(2)}) %all-to-all-start.14) | async-done | bytes 262176 | tf_op jit(solution)/shard_map/all_to_all | solution.py:149
  307.0 2.2 copy-done.2
  309.2 1.6 layer.28
  310.7 9.9 %all_to_all.107.x_ref = bf16[8,128,128]{2,1,0:T(8,128)(2,1)S(1)} all-to-all(bf16[8,128,128]{2,1,0:T(8,128)(2,1)S(1)} %get-tuple-element.67), channel_id=1, replica_groups=mesh['pp'=16,'fs'=4,'tp'=8] {'tp'}, dimensions={0} | all-to-all | bytes 524288 | tf_op jit(solution)/shard_map/all_to_all | solution.py:149
  320.7 1.6 layer.29
  322.3 9.9 %all_to_all.108.x_ref = bf16[8,128,128]{2,1,0:T(8,128)(2,1)S(1)} all-to-all(bf16[8,128,128]{2,1,0:T(8,128)(2,1)S(1)} %get-tuple-element.69), channel_id=1, replica_groups=mesh['pp'=16,'fs'=4,'tp'=8] {'tp'}, dimensions={0} | all-to-all | bytes 524288 | tf_op jit(solution)/shard_map/all_to_all | solution.py:149
  332.2 1.6 layer.30
  333.8 9.9 %all_to_all.109.x_ref = bf16[8,128,128]{2,1,0:T(8,128)(2,1)S(1)} all-to-all(bf16[8,128,128]{2,1,0:T(8,128)(2,1)S(1)} %get-tuple-element.71), channel_id=1, replica_groups=mesh['pp'=16,'fs'=4,'tp'=8] {'tp'}, dimensions={0} | all-to-all | bytes 524288 | tf_op jit(solution)/shard_map/all_to_all | solution.py:149
  343.7 1.6 layer.31
  345.3 9.9 %all_to_all.110 = bf16[8,128,128]{2,1,0:T(8,128)(2,1)S(1)} all-to-all(bf16[8,128,128]{2,1,0:T(8,128)(2,1)S(1)} %get-tuple-element.74), channel_id=1, replica_groups=mesh['pp'=16,'fs'=4,'tp'=8] {'tp'}, dimensions={0} | all-to-all | bytes 524288 | tf_op jit(solution)/shard_map/all_to_all | solution.py:149
  (38 shorter events, 5.5 us)
Async XLA Ops:
  6.5 79.7 %all-gather.10.cloned.1.call-start = ((), (), s32[]{:S(2)}) async-start(), calls=%async_computation.19 | async-start | bytes 4456448 | tf_op jit(solution)/shard_map/all_gather | solution.py:198
  10.6 42.7 %all-to-all-start = ((bf16[8,128,128]{2,1,0:T(8,128)(2,1)}), bf16[8,128,128]{2,1,0:T(8,128)(2,1)S(1)}, u32[]{:S(2)}, u32[]{:S(2)}) async-start(bf16[8,128,128]{2,1,0:T(8,128)(2,1)} %broadcast_in_dim.22), calls=%async_computation | async-start | bytes 524288 | tf_op jit(solution)/shard_map/all_to_all | solution.py:149
  20.7 176.5 %all-gather.12.cloned.1.call-start = ((), (), s32[]{:S(2)}) async-start(), calls=%async_computation.20 | async-start | bytes 5242880 | tf_op jit(solution)/shard_map/all_gather | solution.py:206
  89.3 17.9 %copy-start.6 = (bf16[1,128,128]{2,1,0:T(8,128)(2,1)S(1)}, bf16[1,128,128]{2,1,0:T(8,128)(2,1)}, u32[]{:S(2)}) copy-start(bf16[1,128,128]{2,1,0:T(8,128)(2,1)} %param.11) | copy-start | bytes 98308
  89.3 156.0 %all-gather.14.cloned.1.call-start = ((), (), s32[]{:S(2)}) async-start(), calls=%async_computation.21 | async-start | bytes 6553600 | tf_op jit(solution)/shard_map/all_gather | solution.py:206
  91.9 208.6 %all-gather.16.cloned.1.call-start = ((), (), s32[]{:S(2)}) async-start(), calls=%async_computation.22 | async-start | bytes 5242880 | tf_op jit(solution)/shard_map/all_gather | solution.py:206
  109.5 22.8 %all-to-all-start.2 = ((bf16[8,128,128]{2,1,0:T(8,128)(2,1)}), bf16[8,128,128]{2,1,0:T(8,128)(2,1)S(1)}, u32[]{:S(2)}, u32[]{:S(2)}) async-start(bf16[8,128,128]{2,1,0:T(8,128)(2,1)} %get-tuple-element.43), calls=%async_computation.2 | async-start | bytes 524288 | tf_op jit(solution)/shard_map/all_to_all | solution.py:149
  197.2 2.2 copy-start.4
  199.4 11.5 %copy-start.5 = (bf16[16,256,512]{2,1,0:T(8,128)(2,1)S(1)}, bf16[16,256,512]{2,1,0:T(8,128)(2,1)}, u32[]{:S(2)}) copy-start(bf16[16,256,512]{2,1,0:T(8,128)(2,1)} %all-gather.12.cloned.1.call-done) | copy-start | bytes 12582916
  245.3 2.5 copy-start
  247.8 11.5 %copy-start.1 = (bf16[20,256,512]{2,1,0:T(8,128)(2,1)S(1)}, bf16[20,256,512]{2,1,0:T(8,128)(2,1)}, u32[]{:S(2)}) copy-start(bf16[20,256,512]{2,1,0:T(8,128)(2,1)} %all-gather.14.cloned.1.call-done) | copy-start | bytes 15728644
  296.2 10.8 %all-to-all-start.14 = ((bf16[8,128,128]{2,1,0:T(8,128)(2,1)}), bf16[8,128,128]{2,1,0:T(8,128)(2,1)S(1)}, u32[]{:S(2)}, u32[]{:S(2)}) async-start(bf16[8,128,128]{2,1,0:T(8,128)(2,1)} %get-tuple-element.65), calls=%async_computation.14 | async-start | bytes 524288 | tf_op jit(solution)/shard_map/all_to_all | solution.py:149
  307.0 2.2 copy-start.2
  309.2 11.5 %copy-start.3 = (bf16[16,256,512]{2,1,0:T(8,128)(2,1)S(1)}, bf16[16,256,512]{2,1,0:T(8,128)(2,1)}, u32[]{:S(2)}) copy-start(bf16[16,256,512]{2,1,0:T(8,128)(2,1)} %all-gather.16.cloned.1.call-done) | copy-start | bytes 12582916
  333.8 21.6 %copy-start.7 = (f32[128]{0:T(128)S(1)}, f32[128]{0:T(128)}, u32[]{:S(2)}) copy-start(f32[128]{0:T(128)} %param.21) | copy-start | bytes 1540
Sparse Core Ops, SparseCore 0:
  9.4 76.8 all-gather.9
  89.4 81.0 all-gather.11
  172.6 64.9 all-gather.13
  239.6 56.4 all-gather.15

commit v3 on v2

--- a/solution.py
+++ b/solution.py
@@ -1,3 +1,5 @@
+from functools import partial
+
 import jax
 import jax.numpy as jnp
 from jax import lax
@@ -7,15 +9,15 @@
 
 epsilon = 1e-06
 TILE = 32
-GROUPS = (0, 1, 3, 7, 12, 16)
-DIRECT = 3
+GROUPS = (0, 2, 7, 12, 16)
+DIRECT = 2
 
 
 def silu(a):
     return a / (1.0 + jnp.exp(-a))
 
 
-def layer_kernel(x_ref, own_ref, weight_ref, table_ref, out_ref, copies_ref):
+def layer_kernel(layer, place, x_ref, own_ref, weight_ref, table_ref, out_ref, copies_ref):
     rows, width = own_ref.shape
     parts = weight_ref.shape[0]
     part_width = weight_ref.shape[2]
@@ -29,11 +31,11 @@
     for i in range(parts):
         projected += jnp.dot(
             x[:, i * part_width : (i + 1) * part_width],
-            weight_ref[i, 0],
+            weight_ref[i, place],
             preferred_element_type=f32,
         )
     projected = projected * inv_rms
-    table = table_ref[0]
+    table = table_ref[layer]
     vectors = jnp.concatenate([table, jnp.zeros_like(table)], axis=0).astype(bf16)
     logits = lax.dot_general(vectors, x, contract_lanes, preferred_element_type=f32)
 
@@ -121,20 +123,11 @@
 
 
 def apply_layer(layer, place, everything, own, weights, tables, interpret=False):
-    parts, _, part_width, columns = weights.shape
+    in_vmem = pl.BlockSpec(memory_space=pltpu.VMEM)
     return pl.pallas_call(
-        layer_kernel,
-        grid=(1,),
-        in_specs=[
-            pl.BlockSpec(everything.shape, lambda i: (0, 0, 0)),
-            pl.BlockSpec(own.shape, lambda i: (0, 0)),
-            pl.BlockSpec((parts, 1, part_width, columns), lambda i: (0, place, 0, 0)),
-            pl.BlockSpec((1, *tables.shape[1:]), lambda i: (layer, 0, 0)),
-        ],
-        out_specs=[
-            pl.BlockSpec(own.shape, lambda i: (0, 0)),
-            pl.BlockSpec(everything.shape, lambda i: (0, 0, 0)),
-        ],
+        partial(layer_kernel, layer, place),
+        in_specs=[in_vmem] * 4,
+        out_specs=[in_vmem] * 2,
         out_shape=[
             jax.ShapeDtypeStruct(own.shape, own.dtype),
             jax.ShapeDtypeStruct(everything.shape, own.dtype),
@@ -199,16 +192,18 @@
     quarters, everything, tables = lax.optimization_barrier((quarters, everything, tables))
     stored = {}
     for begin, end in zip(GROUPS[:-1], GROUPS[1:]):
+        if begin > DIRECT:
+            quarters, stored[0] = lax.optimization_barrier((quarters, stored[0]))
         group = quarters[begin:end]
         if begin < DIRECT:
             group = from_everyone(group, "fs")
         else:
             group = lax.all_gather(group, "fs", axis=0)
         for layer in range(begin, end):
-            stored[layer] = (layer - begin, group)
+            stored[layer] = group
     for layer in range(layer_total):
-        place, weights = stored[layer]
-        own, copies = apply_layer(layer, place, everything, own, weights, tables)
+        place = layer - max(begin for begin in GROUPS if begin <= layer)
+        own, copies = apply_layer(layer, place, everything, own, stored[layer], tables)
         everything = exchange(copies, "tp")
     square = everything.astype(jnp.float32)
     row_total = jnp.sum(jnp.sum(square * square, axis=0), axis=1, keepdims=True)

time: 364 us -> 345 us (0.948)
  starting transfers between devices: 30.8 us -> 14.5 us
  waiting for transfers between devices: 45.5 us -> 41.4 us
    all_to_all x3 -> x2, starting transfers between devices: 30.7 us -> 14.4 us  [exchange(): return lax.all_to_all(copies, axis, split_axis=0, concat_axis=0, tiled=True)]
    all_to_all x3 -> x2, waiting for transfers between devices: 11.9 us -> 4.66 us  [exchange(): return lax.all_to_all(copies, axis, split_axis=0, concat_axis=0, tiled=True)]
    all_gather x3, waiting for transfers between devices: 0.01 us -> 3.86 us  [on_device(): group = lax.all_gather(group, 'fs', axis=0)]
  transfers between devices with their start and end apart: 7 -> 6, of which waited for: 3 -> 5; matrix products, arithmetic and copies ran while one was open for 2% -> 3% of each run, Pallas kernels for 6% -> 6%
where the time goes in v3:
time: 345 us; the launch traced here: 343 us
  blocking collectives  225 us (65%)
  waiting for transfers between devices  41.4 us (12%)
  Pallas kernels  26 us (8%)
  local copies, waits for them, and re-layouts  20.5 us (6%)
  starting transfers between devices  14.5 us (4%)
  between operations  14 us (4%)
    all_to_all x16, blocking collectives, exchange(): return lax.all_to_all(copies, axis, split_axis=0, concat_axis=0, tiled=True)  195 us
    all_gather x1, waiting for transfers between devices, on_device(): quarters = lax.all_gather(packed, 'pp', axis=0)  32.8 us
    all_gather x1, blocking collectives, on_device(): tables = lax.all_gather(table, 'pp', axis=0)  29.9 us
    pallas_call x16, Pallas kernels, apply_layer(): pl.pallas_call(partial(layer_kernel, layer, place), in_specs=[in_vmem] *...  26 us
    all_to_all x2, starting transfers between devices, exchange(): return lax.all_to_all(copies, axis, split_axis=0, concat_axis=0, tiled=True)  14.4 us
    slice x4, local copies, waits for them, and re-layouts, on_device(): group = quarters[begin:end]  8.48 us
    unnamed x16, local copies, waits for them, and re-layouts  7.18 us
  transfers between devices with their start and end apart: 6, of which 5 were waited for; matrix products, arithmetic and copies ran while one was open for 3% of the time, Pallas kernels for 6%

profile of v3, /device:TPU:1, one launch (start us, length us, event | category | flops | bytes accessed | tf_op | source)
XLA Modules:
  0.0 343.5 jit_solution(4060824021016794105)
XLA Ops:
  7.4 0.9 dynamic-slice_bitcast_fusion.2
  9.1 1.5 broadcast_in_dim.19
  10.6 10.2 %all-to-all-start = ((bf16[8,128,128]{2,1,0:T(8,128)(2,1)}), bf16[8,128,128]{2,1,0:T(8,128)(2,1)S(1)}, u32[]{:S(2)}, u32[]{:S(2)}) async-start(bf16[8,128,128]{2,1,0:T(8,128)(2,1)} %broadcast_in_dim.19), calls=%async_computation | async-start | bytes 524288 | tf_op jit(solution)/shard_map/all_to_all | solution.py:142
  23.5 29.9 %all-gather.1 = f32[128,1024]{1,0:T(8,128)S(1)} all-gather(f32[8,1024]{1,0:T(8,128)S(1)} %concatenate.7), channel_id=3, replica_groups=mesh['pp'=16,'fs'=4,'tp'=8] {'pp'}, dimensions={0}, use_global_device_ids=true | all-gather | bytes 557056 | tf_op jit(solution)/shard_map/all_gather | solution.py:188
  53.4 32.8 %all-gather.10.cloned.1.call-done = bf16[4096,512]{1,0:T(8,128)(2,1)} async-done(((bf16[256,512]{1,0:T(8,128)(2,1)}), bf16[4096,512]{1,0:T(8,128)(2,1)}) %all-gather.10.cloned.1.call-update) | async-done | bytes 4194320 | tf_op jit(solution)/shard_map/all_gather | solution.py:191
  86.2 2.5 slice.13
  88.8 1.1 slice.12
  90.0 21.8 %all_to_all.90.weight_ref = bf16[4,2,256,512]{3,2,1,0:T(8,128)(2,1)S(1)} all-to-all(bf16[4,2,256,512]{3,2,1,0:T(8,128)(2,1)S(1)} %broadcast_in_dim.22), channel_id=1, replica_groups=mesh['pp'=16,'fs'=4,'tp'=8] {'fs'}, dimensions={0} | all-to-all | bytes 4194304 | tf_op jit(solution)/shard_map/all_to_all | solution.py:142
  111.8 2.6 slice.14
  114.5 2.3 slice.15
  116.8 1.6 layer.16
  118.4 31.4 %all_to_all.91.x_ref = bf16[8,128,128]{2,1,0:T(8,128)(2,1)S(1)} all-to-all(bf16[8,128,128]{2,1,0:T(8,128)(2,1)S(1)} %get-tuple-element.47), channel_id=1, replica_groups=mesh['pp'=16,'fs'=4,'tp'=8] {'tp'}, dimensions={0} | all-to-all | bytes 524288 | tf_op jit(solution)/shard_map/all_to_all | solution.py:142
  149.8 1.6 layer.17
  151.4 9.9 %all_to_all.92.x_ref = bf16[8,128,128]{2,1,0:T(8,128)(2,1)S(1)} all-to-all(bf16[8,128,128]{2,1,0:T(8,128)(2,1)S(1)} %get-tuple-element.49), channel_id=1, replica_groups=mesh['pp'=16,'fs'=4,'tp'=8] {'tp'}, dimensions={0} | all-to-all | bytes 524288 | tf_op jit(solution)/shard_map/all_to_all | solution.py:142
  161.3 1.8 all-gather.12.cloned.1.call-done
  163.0 2.5 copy-done.2
  165.5 1.6 layer.18
  167.1 11.3 %all_to_all.93.x_ref = bf16[8,128,128]{2,1,0:T(8,128)(2,1)S(1)} all-to-all(bf16[8,128,128]{2,1,0:T(8,128)(2,1)S(1)} %get-tuple-element.51), channel_id=1, replica_groups=mesh['pp'=16,'fs'=4,'tp'=8] {'tp'}, dimensions={0} | all-to-all | bytes 524288 | tf_op jit(solution)/shard_map/all_to_all | solution.py:142
  178.4 1.6 layer.19
  180.0 10.0 %all_to_all.94.x_ref = bf16[8,128,128]{2,1,0:T(8,128)(2,1)S(1)} all-to-all(bf16[8,128,128]{2,1,0:T(8,128)(2,1)S(1)} %get-tuple-element.53), channel_id=1, replica_groups=mesh['pp'=16,'fs'=4,'tp'=8] {'tp'}, dimensions={0} | all-to-all | bytes 524288 | tf_op jit(solution)/shard_map/all_to_all | solution.py:142
  190.0 1.6 layer.20
  191.6 9.9 %all_to_all.95.x_ref = bf16[8,128,128]{2,1,0:T(8,128)(2,1)S(1)} all-to-all(bf16[8,128,128]{2,1,0:T(8,128)(2,1)S(1)} %get-tuple-element.55), channel_id=1, replica_groups=mesh['pp'=16,'fs'=4,'tp'=8] {'tp'}, dimensions={0} | all-to-all | bytes 524288 | tf_op jit(solution)/shard_map/all_to_all | solution.py:142
  201.5 1.6 layer.21
  203.1 9.9 %all_to_all.96.x_ref = bf16[8,128,128]{2,1,0:T(8,128)(2,1)S(1)} all-to-all(bf16[8,128,128]{2,1,0:T(8,128)(2,1)S(1)} %get-tuple-element.57), channel_id=1, replica_groups=mesh['pp'=16,'fs'=4,'tp'=8] {'tp'}, dimensions={0} | all-to-all | bytes 524288 | tf_op jit(solution)/shard_map/all_to_all | solution.py:142
  213.0 1.6 layer.22
  214.6 9.9 %all_to_all.97.x_ref = bf16[8,128,128]{2,1,0:T(8,128)(2,1)S(1)} all-to-all(bf16[8,128,128]{2,1,0:T(8,128)(2,1)S(1)} %get-tuple-element.59), channel_id=1, replica_groups=mesh['pp'=16,'fs'=4,'tp'=8] {'tp'}, dimensions={0} | all-to-all | bytes 524288 | tf_op jit(solution)/shard_map/all_to_all | solution.py:142
  224.8 2.5 copy-done
  227.3 1.6 layer.23
  228.8 11.4 %all_to_all.98.x_ref = bf16[8,128,128]{2,1,0:T(8,128)(2,1)S(1)} all-to-all(bf16[8,128,128]{2,1,0:T(8,128)(2,1)S(1)} %get-tuple-element.62), channel_id=1, replica_groups=mesh['pp'=16,'fs'=4,'tp'=8] {'tp'}, dimensions={0} | all-to-all | bytes 524288 | tf_op jit(solution)/shard_map/all_to_all | solution.py:142
  240.2 1.6 layer.24
  241.8 10.0 %all_to_all.99.x_ref = bf16[8,128,128]{2,1,0:T(8,128)(2,1)S(1)} all-to-all(bf16[8,128,128]{2,1,0:T(8,128)(2,1)S(1)} %get-tuple-element.64), channel_id=1, replica_groups=mesh['pp'=16,'fs'=4,'tp'=8] {'tp'}, dimensions={0} | all-to-all | bytes 524288 | tf_op jit(solution)/shard_map/all_to_all | solution.py:142
  251.8 1.6 layer.25
  253.4 9.9 %all_to_all.100.x_ref = bf16[8,128,128]{2,1,0:T(8,128)(2,1)S(1)} all-to-all(bf16[8,128,128]{2,1,0:T(8,128)(2,1)S(1)} %get-tuple-element.66), channel_id=1, replica_groups=mesh['pp'=16,'fs'=4,'tp'=8] {'tp'}, dimensions={0} | all-to-all | bytes 524288 | tf_op jit(solution)/shard_map/all_to_all | solution.py:142
  263.3 1.6 layer.26
  264.9 9.9 %all_to_all.101.x_ref = bf16[8,128,128]{2,1,0:T(8,128)(2,1)S(1)} all-to-all(bf16[8,128,128]{2,1,0:T(8,128)(2,1)S(1)} %get-tuple-element.68), channel_id=1, replica_groups=mesh['pp'=16,'fs'=4,'tp'=8] {'tp'}, dimensions={0} | all-to-all | bytes 524288 | tf_op jit(solution)/shard_map/all_to_all | solution.py:142
  274.8 2.3 layer.27
  277.1 4.3 %all-to-all-start.13 = ((bf16[8,128,128]{2,1,0:T(8,128)(2,1)}), bf16[8,128,128]{2,1,0:T(8,128)(2,1)S(1)}, u32[]{:S(2)}, u32[]{:S(2)}) async-start(bf16[8,128,128]{2,1,0:T(8,128)(2,1)} %get-tuple-element.70), calls=%async_computation.13 | async-start | bytes 524288 | tf_op jit(solution)/shard_map/all_to_all | solution.py:142
  281.4 1.8 all-gather.16.cloned.1.call-done
  283.2 4.7 %all-to-all-done.13.x_ref = bf16[8,128,128]{2,1,0:T(8,128)(2,1)S(1)} async-done(((bf16[8,128,128]{2,1,0:T(8,128)(2,1)}), bf16[8,128,128]{2,1,0:T(8,128)(2,1)S(1)}, u32[]{:S(2)}, u32[]{:S(2)}) %all-to-all-start.13) | async-done | bytes 262176 | tf_op jit(solution)/shard_map/all_to_all | solution.py:142
  287.9 2.2 copy-done.4
  290.1 1.6 layer.28
  291.7 9.9 %all_to_all.102.x_ref = bf16[8,128,128]{2,1,0:T(8,128)(2,1)S(1)} all-to-all(bf16[8,128,128]{2,1,0:T(8,128)(2,1)S(1)} %get-tuple-element.73), channel_id=1, replica_groups=mesh['pp'=16,'fs'=4,'tp'=8] {'tp'}, dimensions={0} | all-to-all | bytes 524288 | tf_op jit(solution)/shard_map/all_to_all | solution.py:142
  301.6 1.6 layer.29
  303.2 9.9 %all_to_all.103.x_ref = bf16[8,128,128]{2,1,0:T(8,128)(2,1)S(1)} all-to-all(bf16[8,128,128]{2,1,0:T(8,128)(2,1)S(1)} %get-tuple-element.75), channel_id=1, replica_groups=mesh['pp'=16,'fs'=4,'tp'=8] {'tp'}, dimensions={0} | all-to-all | bytes 524288 | tf_op jit(solution)/shard_map/all_to_all | solution.py:142
  313.1 1.6 layer.30
  314.7 9.9 %all_to_all.104.x_ref = bf16[8,128,128]{2,1,0:T(8,128)(2,1)S(1)} all-to-all(bf16[8,128,128]{2,1,0:T(8,128)(2,1)S(1)} %get-tuple-element.77), channel_id=1, replica_groups=mesh['pp'=16,'fs'=4,'tp'=8] {'tp'}, dimensions={0} | all-to-all | bytes 524288 | tf_op jit(solution)/shard_map/all_to_all | solution.py:142
  324.6 1.6 layer.31
  326.2 9.9 %all_to_all.105 = bf16[8,128,128]{2,1,0:T(8,128)(2,1)S(1)} all-to-all(bf16[8,128,128]{2,1,0:T(8,128)(2,1)S(1)} %get-tuple-element.80), channel_id=1, replica_groups=mesh['pp'=16,'fs'=4,'tp'=8] {'tp'}, dimensions={0} | all-to-all | bytes 524288 | tf_op jit(solution)/shard_map/all_to_all | solution.py:142
  (35 shorter events, 5.2 us)
Async XLA Ops:
  6.5 79.6 %all-gather.10.cloned.1.call-start = ((), (), s32[]{:S(2)}) async-start(), calls=%async_computation.18 | async-start | bytes 4456448 | tf_op jit(solution)/shard_map/all_gather | solution.py:191
  10.6 42.8 %all-to-all-start = ((bf16[8,128,128]{2,1,0:T(8,128)(2,1)}), bf16[8,128,128]{2,1,0:T(8,128)(2,1)S(1)}, u32[]{:S(2)}, u32[]{:S(2)}) async-start(bf16[8,128,128]{2,1,0:T(8,128)(2,1)} %broadcast_in_dim.19), calls=%async_computation | async-start | bytes 524288 | tf_op jit(solution)/shard_map/all_to_all | solution.py:142
  20.7 142.3 %all-gather.12.cloned.1.call-start = ((), (), s32[]{:S(2)}) async-start(), calls=%async_computation.19 | async-start | bytes 6553600 | tf_op jit(solution)/shard_map/all_gather | solution.py:201
  88.7 136.0 %all-gather.14.cloned.1.call-start = ((), (), s32[]{:S(2)}) async-start(), calls=%async_computation.20 | async-start | bytes 6553600 | tf_op jit(solution)/shard_map/all_gather | solution.py:201
  111.8 5.0 %copy-start.6 = (bf16[1,128,128]{2,1,0:T(8,128)(2,1)S(1)}, bf16[1,128,128]{2,1,0:T(8,128)(2,1)}, u32[]{:S(2)}) copy-start(bf16[1,128,128]{2,1,0:T(8,128)(2,1)} %param.11) | copy-start | bytes 98308
  114.4 168.8 %all-gather.16.cloned.1.call-start = ((), (), s32[]{:S(2)}) async-start(), calls=%async_computation.21 | async-start | bytes 5242880 | tf_op jit(solution)/shard_map/all_gather | solution.py:201
  163.0 2.5 copy-start.2
  165.5 12.9 %copy-start.3 = (bf16[20,256,512]{2,1,0:T(8,128)(2,1)S(1)}, bf16[20,256,512]{2,1,0:T(8,128)(2,1)}, u32[]{:S(2)}) copy-start(bf16[20,256,512]{2,1,0:T(8,128)(2,1)} %all-gather.12.cloned.1.call-done) | copy-start | bytes 15728644
  224.8 2.5 copy-start
  227.3 13.0 %copy-start.1 = (bf16[20,256,512]{2,1,0:T(8,128)(2,1)S(1)}, bf16[20,256,512]{2,1,0:T(8,128)(2,1)}, u32[]{:S(2)}) copy-start(bf16[20,256,512]{2,1,0:T(8,128)(2,1)} %all-gather.14.cloned.1.call-done) | copy-start | bytes 15728644
  277.1 10.8 %all-to-all-start.13 = ((bf16[8,128,128]{2,1,0:T(8,128)(2,1)}), bf16[8,128,128]{2,1,0:T(8,128)(2,1)S(1)}, u32[]{:S(2)}, u32[]{:S(2)}) async-start(bf16[8,128,128]{2,1,0:T(8,128)(2,1)} %get-tuple-element.70), calls=%async_computation.13 | async-start | bytes 524288 | tf_op jit(solution)/shard_map/all_to_all | solution.py:142
  287.9 2.2 copy-start.4
  290.1 11.5 %copy-start.5 = (bf16[16,256,512]{2,1,0:T(8,128)(2,1)S(1)}, bf16[16,256,512]{2,1,0:T(8,128)(2,1)}, u32[]{:S(2)}) copy-start(bf16[16,256,512]{2,1,0:T(8,128)(2,1)} %all-gather.16.cloned.1.call-done) | copy-start | bytes 12582916
  314.7 21.6 %copy-start.7 = (f32[128]{0:T(128)S(1)}, f32[128]{0:T(128)}, u32[]{:S(2)}) copy-start(f32[128]{0:T(128)} %param.21) | copy-start | bytes 1540
Sparse Core Ops, SparseCore 0:
  9.4 76.7 all-gather.9
  88.9 74.1 all-gather.11
  165.1 59.5 all-gather.13
  226.7 56.4 all-gather.15

commit v4 on v3

--- a/solution.py
+++ b/solution.py
@@ -17,7 +17,27 @@
     return a / (1.0 + jnp.exp(-a))
 
 
+def fetching_kernel(
+    layer, place, x_ref, own_ref, remote_ref, table_ref, out_ref, copies_ref, weight_ref, sems
+):
+    pieces = [
+        pltpu.make_async_copy(remote_ref.at[i, place], weight_ref.at[i, 0], sems.at[i])
+        for i in range(remote_ref.shape[0])
+    ]
+    for piece in pieces:
+        piece.start()
+    layer_body(
+        layer, 0, pieces, x_ref, own_ref, weight_ref, table_ref, out_ref, copies_ref
+    )
+
+
 def layer_kernel(layer, place, x_ref, own_ref, weight_ref, table_ref, out_ref, copies_ref):
+    layer_body(layer, place, (), x_ref, own_ref, weight_ref, table_ref, out_ref, copies_ref)
+
+
+def layer_body(
+    layer, place, pieces, x_ref, own_ref, weight_ref, table_ref, out_ref, copies_ref
+):
     rows, width = own_ref.shape
     parts = weight_ref.shape[0]
     part_width = weight_ref.shape[2]
@@ -29,6 +49,8 @@
     inv_rms = lax.rsqrt(jnp.sum(x32 * x32, axis=1, keepdims=True) * (1.0 / model_width) + epsilon)
     projected = jnp.zeros((rows, weight_ref.shape[3]), f32)
     for i in range(parts):
+        if pieces:
+            pieces[i].wait()
         projected += jnp.dot(
             x[:, i * part_width : (i + 1) * part_width],
             weight_ref[i, place],
@@ -122,11 +144,18 @@
         copies_ref[i] = updated
 
 
-def apply_layer(layer, place, everything, own, weights, tables, interpret=False):
+def apply_layer(layer, place, fetch, everything, own, weights, tables, interpret=False):
     in_vmem = pl.BlockSpec(memory_space=pltpu.VMEM)
+    anywhere = pl.BlockSpec(memory_space=pltpu.HBM)
+    parts, _, part_width, columns = weights.shape
+    scratch = [
+        pltpu.VMEM((parts, 1, part_width, columns), weights.dtype),
+        pltpu.SemaphoreType.DMA((parts,)),
+    ]
     return pl.pallas_call(
-        partial(layer_kernel, layer, place),
-        in_specs=[in_vmem] * 4,
+        partial(fetching_kernel if fetch else layer_kernel, layer, place),
+        scratch_shapes=scratch if fetch else [],
+        in_specs=[in_vmem, in_vmem, anywhere if fetch else in_vmem, in_vmem],
         out_specs=[in_vmem] * 2,
         out_shape=[
             jax.ShapeDtypeStruct(own.shape, own.dtype),
@@ -203,7 +232,17 @@
             stored[layer] = group
     for layer in range(layer_total):
         place = layer - max(begin for begin in GROUPS if begin <= layer)
-        own, copies = apply_layer(layer, place, everything, own, stored[layer], tables)
+        fetch = layer in GROUPS and layer >= DIRECT
+        if fetch:
+            group, everything = lax.optimization_barrier((stored[layer], everything))
+            for later in range(layer, layer_total):
+                if stored[later] is stored[layer] and later != layer:
+                    stored[later] = group
+            stored[layer] = group
+        weights = stored[layer]
+        if fetch:
+            weights = pltpu.with_memory_space_constraint(weights, pltpu.HBM)
+        own, copies = apply_layer(layer, place, fetch, everything, own, weights, tables)
         everything = exchange(copies, "tp")
     square = everything.astype(jnp.float32)
     row_total = jnp.sum(jnp.sum(square * square, axis=0), axis=1, keepdims=True)

time: 345 us -> 343 us (level)
  local copies, waits for them, and re-layouts: 20.5 us -> 13.3 us
  Pallas kernels: 26 us -> 29.9 us
    unnamed x16 -> x10, local copies, waits for them, and re-layouts: 7.18 us -> 0.02 us
    pallas_call x16, Pallas kernels: 26 us -> 29.9 us  [apply_layer(): pl.pallas_call(partial(fetching_kernel if fetch else layer_kernel, layer,...]
  transfers between devices with their start and end apart: 6 -> 6, of which waited for: 5 -> 5; matrix products, arithmetic and copies ran while one was open for 3% -> 3% of each run, Pallas kernels for 6% -> 7%
where the time goes in v4:
time: 343 us; the launch traced here: 341 us
  blocking collectives  224 us (65%)
  waiting for transfers between devices  43.3 us (13%)
  Pallas kernels  29.9 us (9%)
  starting transfers between devices  14.5 us (4%)
  between operations  14 us (4%)
  local copies, waits for them, and re-layouts  13.3 us (4%)
    all_to_all x16, blocking collectives, exchange(): return lax.all_to_all(copies, axis, split_axis=0, concat_axis=0, tiled=True)  194 us
    all_gather x1, waiting for transfers between devices, on_device(): quarters = lax.all_gather(packed, 'pp', axis=0)  33 us
    pallas_call x16, Pallas kernels, apply_layer(): pl.pallas_call(partial(fetching_kernel if fetch else layer_kernel, layer,...  29.9 us
    all_gather x1, blocking collectives, on_device(): tables = lax.all_gather(table, 'pp', axis=0)  29.8 us
    all_to_all x2, starting transfers between devices, exchange(): return lax.all_to_all(copies, axis, split_axis=0, concat_axis=0, tiled=True)  14.4 us
    slice x4, local copies, waits for them, and re-layouts, on_device(): group = quarters[begin:end]  8.48 us
  transfers between devices with their start and end apart: 6, of which 5 were waited for; matrix products, arithmetic and copies ran while one was open for 3% of the time, Pallas kernels for 7%

profile of v4, /device:TPU:1, one launch (start us, length us, event | category | flops | bytes accessed | tf_op | source)
XLA Modules:
  0.0 341.4 jit_solution(4858263916501979988)
XLA Ops:
  6.5 0.9 dynamic-slice_bitcast_fusion
  7.4 0.9 dynamic-slice_bitcast_fusion.2
  8.3 0.7 pad_maximum_fusion
  9.1 1.5 broadcast_in_dim.19
  10.6 10.2 %all-to-all-start = ((bf16[8,128,128]{2,1,0:T(8,128)(2,1)}), bf16[8,128,128]{2,1,0:T(8,128)(2,1)S(1)}, u32[]{:S(2)}, u32[]{:S(2)}) async-start(bf16[8,128,128]{2,1,0:T(8,128)(2,1)} %broadcast_in_dim.19), calls=%async_computation | async-start | bytes 524288 | tf_op jit(solution)/shard_map/all_to_all | solution.py:171
  23.5 29.8 %all-gather.1 = f32[128,1024]{1,0:T(8,128)S(1)} all-gather(f32[8,1024]{1,0:T(8,128)S(1)} %concatenate.7), channel_id=3, replica_groups=mesh['pp'=16,'fs'=4,'tp'=8] {'pp'}, dimensions={0}, use_global_device_ids=true | all-gather | bytes 557056 | tf_op jit(solution)/shard_map/all_gather | solution.py:217
  53.3 33.0 %all-gather.10.cloned.1.call-done = bf16[4096,512]{1,0:T(8,128)(2,1)} async-done(((bf16[256,512]{1,0:T(8,128)(2,1)}), bf16[4096,512]{1,0:T(8,128)(2,1)}) %all-gather.10.cloned.1.call-update) | async-done | bytes 4194320 | tf_op jit(solution)/shard_map/all_gather | solution.py:220
  86.2 2.5 slice.15
  88.8 1.1 slice.12
  90.1 21.7 %all_to_all.90.weight_ref = bf16[4,2,256,512]{3,2,1,0:T(8,128)(2,1)S(1)} all-to-all(bf16[4,2,256,512]{3,2,1,0:T(8,128)(2,1)S(1)} %broadcast_in_dim.22), channel_id=1, replica_groups=mesh['pp'=16,'fs'=4,'tp'=8] {'fs'}, dimensions={0} | all-to-all | bytes 4194304 | tf_op jit(solution)/shard_map/all_to_all | solution.py:171
  111.8 2.6 slice.14
  114.4 2.3 slice.13
  116.8 1.6 layer.16
  118.4 31.1 %all_to_all.91.x_ref = bf16[8,128,128]{2,1,0:T(8,128)(2,1)S(1)} all-to-all(bf16[8,128,128]{2,1,0:T(8,128)(2,1)S(1)} %get-tuple-element.55), channel_id=1, replica_groups=mesh['pp'=16,'fs'=4,'tp'=8] {'tp'}, dimensions={0} | all-to-all | bytes 524288 | tf_op jit(solution)/shard_map/all_to_all | solution.py:171
  149.5 1.6 layer.17
  151.1 9.9 %all_to_all.92.x_ref = bf16[8,128,128]{2,1,0:T(8,128)(2,1)S(1)} all-to-all(bf16[8,128,128]{2,1,0:T(8,128)(2,1)S(1)} %get-tuple-element.57), channel_id=1, replica_groups=mesh['pp'=16,'fs'=4,'tp'=8] {'tp'}, dimensions={0} | all-to-all | bytes 524288 | tf_op jit(solution)/shard_map/all_to_all | solution.py:171
  161.0 2.1 all-gather.16.cloned.1.call-done
  163.1 2.9 layer.18
  166.0 11.1 %all_to_all.93.x_ref = bf16[8,128,128]{2,1,0:T(8,128)(2,1)S(1)} all-to-all(bf16[8,128,128]{2,1,0:T(8,128)(2,1)S(1)} %get-tuple-element.61), channel_id=1, replica_groups=mesh['pp'=16,'fs'=4,'tp'=8] {'tp'}, dimensions={0} | all-to-all | bytes 524288 | tf_op jit(solution)/shard_map/all_to_all | solution.py:171
  177.2 1.6 layer.19
  178.8 10.0 %all_to_all.94.x_ref = bf16[8,128,128]{2,1,0:T(8,128)(2,1)S(1)} all-to-all(bf16[8,128,128]{2,1,0:T(8,128)(2,1)S(1)} %get-tuple-element.63), channel_id=1, replica_groups=mesh['pp'=16,'fs'=4,'tp'=8] {'tp'}, dimensions={0} | all-to-all | bytes 524288 | tf_op jit(solution)/shard_map/all_to_all | solution.py:171
  188.7 1.6 layer.20
  190.3 9.9 %all_to_all.95.x_ref = bf16[8,128,128]{2,1,0:T(8,128)(2,1)S(1)} all-to-all(bf16[8,128,128]{2,1,0:T(8,128)(2,1)S(1)} %get-tuple-element.65), channel_id=1, replica_groups=mesh['pp'=16,'fs'=4,'tp'=8] {'tp'}, dimensions={0} | all-to-all | bytes 524288 | tf_op jit(solution)/shard_map/all_to_all | solution.py:171
  200.2 1.6 layer.21
  201.8 9.9 %all_to_all.96.x_ref = bf16[8,128,128]{2,1,0:T(8,128)(2,1)S(1)} all-to-all(bf16[8,128,128]{2,1,0:T(8,128)(2,1)S(1)} %get-tuple-element.67), channel_id=1, replica_groups=mesh['pp'=16,'fs'=4,'tp'=8] {'tp'}, dimensions={0} | all-to-all | bytes 524288 | tf_op jit(solution)/shard_map/all_to_all | solution.py:171
  211.8 1.6 layer.22
  213.3 9.9 %all_to_all.97.x_ref = bf16[8,128,128]{2,1,0:T(8,128)(2,1)S(1)} all-to-all(bf16[8,128,128]{2,1,0:T(8,128)(2,1)S(1)} %get-tuple-element.69), channel_id=1, replica_groups=mesh['pp'=16,'fs'=4,'tp'=8] {'tp'}, dimensions={0} | all-to-all | bytes 524288 | tf_op jit(solution)/shard_map/all_to_all | solution.py:171
  223.3 1.6 all-gather.14.cloned.1.call-done
  224.9 2.9 layer.23
  227.8 11.3 %all_to_all.98.x_ref = bf16[8,128,128]{2,1,0:T(8,128)(2,1)S(1)} all-to-all(bf16[8,128,128]{2,1,0:T(8,128)(2,1)S(1)} %get-tuple-element.73), channel_id=1, replica_groups=mesh['pp'=16,'fs'=4,'tp'=8] {'tp'}, dimensions={0} | all-to-all | bytes 524288 | tf_op jit(solution)/shard_map/all_to_all | solution.py:171
  239.0 1.6 layer.24
  240.6 10.0 %all_to_all.99.x_ref = bf16[8,128,128]{2,1,0:T(8,128)(2,1)S(1)} all-to-all(bf16[8,128,128]{2,1,0:T(8,128)(2,1)S(1)} %get-tuple-element.75), channel_id=1, replica_groups=mesh['pp'=16,'fs'=4,'tp'=8] {'tp'}, dimensions={0} | all-to-all | bytes 524288 | tf_op jit(solution)/shard_map/all_to_all | solution.py:171
  250.6 1.6 layer.25
  252.2 9.9 %all_to_all.100.x_ref = bf16[8,128,128]{2,1,0:T(8,128)(2,1)S(1)} all-to-all(bf16[8,128,128]{2,1,0:T(8,128)(2,1)S(1)} %get-tuple-element.77), channel_id=1, replica_groups=mesh['pp'=16,'fs'=4,'tp'=8] {'tp'}, dimensions={0} | all-to-all | bytes 524288 | tf_op jit(solution)/shard_map/all_to_all | solution.py:171
  262.1 1.6 layer.26
  263.7 9.9 %all_to_all.101.x_ref = bf16[8,128,128]{2,1,0:T(8,128)(2,1)S(1)} all-to-all(bf16[8,128,128]{2,1,0:T(8,128)(2,1)S(1)} %get-tuple-element.79), channel_id=1, replica_groups=mesh['pp'=16,'fs'=4,'tp'=8] {'tp'}, dimensions={0} | all-to-all | bytes 524288 | tf_op jit(solution)/shard_map/all_to_all | solution.py:171
  273.6 2.3 layer.27
  275.9 4.3 %all-to-all-start.13 = ((bf16[8,128,128]{2,1,0:T(8,128)(2,1)}), bf16[8,128,128]{2,1,0:T(8,128)(2,1)S(1)}, u32[]{:S(2)}, u32[]{:S(2)}) async-start(bf16[8,128,128]{2,1,0:T(8,128)(2,1)} %get-tuple-element.81), calls=%async_computation.13 | async-start | bytes 524288 | tf_op jit(solution)/shard_map/all_to_all | solution.py:171
  280.2 3.1 all-gather.12.cloned.1.call-done
  283.3 3.4 %all-to-all-done.13.x_ref = bf16[8,128,128]{2,1,0:T(8,128)(2,1)S(1)} async-done(((bf16[8,128,128]{2,1,0:T(8,128)(2,1)}), bf16[8,128,128]{2,1,0:T(8,128)(2,1)S(1)}, u32[]{:S(2)}, u32[]{:S(2)}) %all-to-all-start.13) | async-done | bytes 262176 | tf_op jit(solution)/shard_map/all_to_all | solution.py:171
  286.7 2.9 layer.28
  289.6 9.9 %all_to_all.102.x_ref = bf16[8,128,128]{2,1,0:T(8,128)(2,1)S(1)} all-to-all(bf16[8,128,128]{2,1,0:T(8,128)(2,1)S(1)} %get-tuple-element.85), channel_id=1, replica_groups=mesh['pp'=16,'fs'=4,'tp'=8] {'tp'}, dimensions={0} | all-to-all | bytes 524288 | tf_op jit(solution)/shard_map/all_to_all | solution.py:171
  299.5 1.6 layer.29
  301.1 9.9 %all_to_all.103.x_ref = bf16[8,128,128]{2,1,0:T(8,128)(2,1)S(1)} all-to-all(bf16[8,128,128]{2,1,0:T(8,128)(2,1)S(1)} %get-tuple-element.87), channel_id=1, replica_groups=mesh['pp'=16,'fs'=4,'tp'=8] {'tp'}, dimensions={0} | all-to-all | bytes 524288 | tf_op jit(solution)/shard_map/all_to_all | solution.py:171
  311.0 1.6 layer.30
  312.6 9.9 %all_to_all.104.x_ref = bf16[8,128,128]{2,1,0:T(8,128)(2,1)S(1)} all-to-all(bf16[8,128,128]{2,1,0:T(8,128)(2,1)S(1)} %get-tuple-element.89), channel_id=1, replica_groups=mesh['pp'=16,'fs'=4,'tp'=8] {'tp'}, dimensions={0} | all-to-all | bytes 524288 | tf_op jit(solution)/shard_map/all_to_all | solution.py:171
  322.5 1.6 layer.31
  324.1 9.9 %all_to_all.105 = bf16[8,128,128]{2,1,0:T(8,128)(2,1)S(1)} all-to-all(bf16[8,128,128]{2,1,0:T(8,128)(2,1)S(1)} %get-tuple-element.92), channel_id=1, replica_groups=mesh['pp'=16,'fs'=4,'tp'=8] {'tp'}, dimensions={0} | all-to-all | bytes 524288 | tf_op jit(solution)/shard_map/all_to_all | solution.py:171
  (29 shorter events, 3.3 us)
Async XLA Ops:
  6.5 79.7 %all-gather.10.cloned.1.call-start = ((), (), s32[]{:S(2)}) async-start(), calls=%async_computation.18 | async-start | bytes 4456448 | tf_op jit(solution)/shard_map/all_gather | solution.py:220
  10.6 42.7 %all-to-all-start = ((bf16[8,128,128]{2,1,0:T(8,128)(2,1)}), bf16[8,128,128]{2,1,0:T(8,128)(2,1)S(1)}, u32[]{:S(2)}, u32[]{:S(2)}) async-start(bf16[8,128,128]{2,1,0:T(8,128)(2,1)} %broadcast_in_dim.19), calls=%async_computation | async-start | bytes 524288 | tf_op jit(solution)/shard_map/all_to_all | solution.py:171
  20.7 142.4 %all-gather.16.cloned.1.call-start = ((), (), s32[]{:S(2)}) async-start(), calls=%async_computation.21 | async-start | bytes 6553600 | tf_op jit(solution)/shard_map/all_gather | solution.py:230
  88.8 136.1 %all-gather.14.cloned.1.call-start = ((), (), s32[]{:S(2)}) async-start(), calls=%async_computation.20 | async-start | bytes 6553600 | tf_op jit(solution)/shard_map/all_gather | solution.py:230
  111.8 5.0 %copy-start.3 = (bf16[1,128,128]{2,1,0:T(8,128)(2,1)S(1)}, bf16[1,128,128]{2,1,0:T(8,128)(2,1)}, u32[]{:S(2)}) copy-start(bf16[1,128,128]{2,1,0:T(8,128)(2,1)} %param.11) | copy-start | bytes 98308
  114.4 168.9 %all-gather.12.cloned.1.call-start = ((), (), s32[]{:S(2)}) async-start(), calls=%async_computation.19 | async-start | bytes 5242880 | tf_op jit(solution)/shard_map/all_gather | solution.py:230
  163.1 14.0 %copy-start.1 = (bf16[20,256,512]{2,1,0:T(8,128)(2,1)S(1)}, bf16[20,256,512]{2,1,0:T(8,128)(2,1)}, u32[]{:S(2)}) copy-start(bf16[20,256,512]{2,1,0:T(8,128)(2,1)} %all-gather.16.cloned.1.call-done) | copy-start | bytes 15728644
  224.9 14.2 %copy-start = (bf16[20,256,512]{2,1,0:T(8,128)(2,1)S(1)}, bf16[20,256,512]{2,1,0:T(8,128)(2,1)}, u32[]{:S(2)}) copy-start(bf16[20,256,512]{2,1,0:T(8,128)(2,1)} %all-gather.14.cloned.1.call-done) | copy-start | bytes 15728644
  275.9 10.8 %all-to-all-start.13 = ((bf16[8,128,128]{2,1,0:T(8,128)(2,1)}), bf16[8,128,128]{2,1,0:T(8,128)(2,1)S(1)}, u32[]{:S(2)}, u32[]{:S(2)}) async-start(bf16[8,128,128]{2,1,0:T(8,128)(2,1)} %get-tuple-element.81), calls=%async_computation.13 | async-start | bytes 524288 | tf_op jit(solution)/shard_map/all_to_all | solution.py:171
  286.7 12.8 %copy-start.2 = (bf16[16,256,512]{2,1,0:T(8,128)(2,1)S(1)}, bf16[16,256,512]{2,1,0:T(8,128)(2,1)}, u32[]{:S(2)}) copy-start(bf16[16,256,512]{2,1,0:T(8,128)(2,1)} %all-gather.12.cloned.1.call-done) | copy-start | bytes 12582916
  312.6 21.6 %copy-start.4 = (f32[128]{0:T(128)S(1)}, f32[128]{0:T(128)}, u32[]{:S(2)}) copy-start(f32[128]{0:T(128)} %param.21) | copy-start | bytes 1540
Sparse Core Ops, SparseCore 0:
  9.4 76.7 all-gather.9
  88.9 74.1 all-gather.15
  165.2 59.5 all-gather.13
  226.8 56.4 all-gather.11
